TPU v7x, 32 devices: a whole 2x2x4 slice. The times are simulated.
32 devices in a mesh: ep: 8 (over z, core), tp: 4 (over y, x).
Axes of the slice: x: 2, y: 2, z: 4, core: 2. Of those that a mesh axis runs over, the one named last changes fastest.
Arguments:
- mix_in: bfloat16 [1024, 2048], P('ep'), may hold values from -6 to 6
- mix_gain: float32 [2048], replicated, may hold values from 0.1 to 1.9
- lam_re: float32 [128, 64], P('tp'), may hold values from -0.34 to -1e-05
- lam_im: float32 [128, 64], P('tp'), may hold values from 0.2 to 4
- log_dt: float32 [128], P('tp'), may hold values from -2.31 to 0
- b_re: float32 [128, 64, 16], P('tp'), may hold values from -0.125 to 0.125
- b_im: float32 [128, 64, 16], P('tp'), may hold values from -0.125 to 0.125
- c_re: float32 [128, 16, 64], P('tp'), may hold values from -0.5 to 0.5
- c_im: float32 [128, 16, 64], P('tp'), may hold values from -0.5 to 0.5
- d_skip: float32 [2048], P('tp'), may hold values from -2 to 2
- log_retain: float32 [1024, 128], P('ep', 'tp'), may hold values from -2.2 to 0
- w_lin: bfloat16 [2048, 2048], P(None, 'tp'), may hold values from -0.125 to 0.125
- w_glu: bfloat16 [2048, 2048], P(None, 'tp'), may hold values from -0.125 to 0.125
- moe_in: bfloat16 [1024, 2048], P('ep'), may hold values from -6 to 6
- moe_gain: float32 [2048], replicated, may hold values from 0.1 to 1.9
- routes: int32 [1024, 2], P('ep'), may hold values from 0 to 7, all different within a row; in each aligned block of 128 rows (0 to 127, 128 to 255, ...) at most 48 rows name the same one
- route_weight: float32 [1024, 2], P('ep'), may hold values from 0.1 to 1
- w_gate: bfloat16 [8, 2048, 4096], P('ep', None, 'tp'), may hold values from -0.125 to 0.125
- w_up: bfloat16 [8, 2048, 4096], P('ep', None, 'tp'), may hold values from -0.125 to 0.125
- w_down: bfloat16 [8, 4096, 2048], P('ep', 'tp'), may hold values from -0.09375 to 0.09375
Outputs:
- mix_out: bfloat16 [1024, 2048], P('ep', 'tp')
- moe_out: bfloat16 [1024, 2048], P('ep', 'tp')
Inputs may be any that keep to these rules, and one draw needn't show every extreme that they name: `routes`: each row names 2 different experts. In each aligned block of 128 rows (the rows of one index of ep) no expert is named by more than 48 rows, and in some block an expert is named by exactly 48 rows.
All inputs are finite; a program needn't handle non-finite values.
Results may differ from a plain program's by a relative error of at most 0.015.
Values may be sent and summed in bfloat16 or wider, within the bound.
A program may use at most 192 MiB of HBM per device.

v0:
```python
import jax
import jax.numpy as jnp
from jax import lax
from jax.sharding import PartitionSpec as P

EPS = 1e-06
HIGHEST = lax.Precision.HIGHEST


def prefix(value, axis, join, neutral):
    count, mine = (lax.axis_size(axis), lax.axis_index(axis))
    pieces = jax.tree.map(lambda part: lax.all_gather(part, axis), value)
    subtotal = jax.tree.map(
        lambda part, zero: jnp.full_like(part, 0) + jnp.asarray(zero, part.dtype), value, neutral
    )

    def turn(position, subtotal):
        longer = join(subtotal, jax.tree.map(lambda part: part[position], pieces))
        return jax.tree.map(lambda new, old: jnp.where(position < mine, new, old), longer, subtotal)

    return lax.fori_loop(0, count - 1, turn, subtotal)


def root_mean_normed(values, gain):
    broadened_rows = values.astype(jnp.float32)
    inverse = lax.rsqrt(jnp.mean(broadened_rows * broadened_rows, axis=-1, keepdims=True) + EPS)
    return (broadened_rows * inverse * gain).astype(jnp.bfloat16)


def compose(earlier, later):
    early_re, early_im, shift_re, shift_im = earlier
    late_re, late_im, offset_re, offset_im = later
    return (
        late_re * early_re - late_im * early_im,
        late_re * early_im + late_im * early_re,
        late_re * shift_re - late_im * shift_im + offset_re,
        late_re * shift_im + late_im * shift_re + offset_im,
    )


def discretize(lam_re, lam_im, log_dt, b_re, b_im):
    time_step = jnp.exp(log_dt)[:, None]
    log_mag = lam_re * time_step
    angle = lam_im * time_step
    half_sine = jnp.sin(0.5 * angle)
    minus_re = jnp.expm1(log_mag) * jnp.cos(angle) - 2.0 * half_sine * half_sine
    minus_im = jnp.exp(log_mag) * jnp.sin(angle)
    denom = lam_re * lam_re + lam_im * lam_im
    coef_re = (minus_re * lam_re + minus_im * lam_im) / denom
    coef_im = (minus_im * lam_re - minus_re * lam_im) / denom
    drive_re = coef_re[..., None] * b_re - coef_im[..., None] * b_im
    drive_im = coef_re[..., None] * b_im + coef_im[..., None] * b_re
    return (log_mag, angle, drive_re, drive_im)


def local_scan(inputs, retain, log_mag, angle, drive_re, drive_im):
    length = inputs.shape[0]
    groups, states, channels = drive_re.shape
    broadened_rows = inputs.astype(jnp.float32).reshape(length, groups, channels)
    push_re = jnp.einsum("tgn,gpn->tgp", broadened_rows, drive_re, precision=HIGHEST).reshape(
        length, groups * states
    )
    push_im = jnp.einsum("tgn,gpn->tgp", broadened_rows, drive_im, precision=HIGHEST).reshape(
        length, groups * states
    )
    magnitude = jnp.exp(log_mag[None] + retain[:, :, None]).reshape(length, groups * states)
    decay_re = magnitude * jnp.cos(angle).reshape(1, groups * states)
    decay_im = magnitude * jnp.sin(angle).reshape(1, groups * states)
    return lax.associative_scan(compose, (decay_re, decay_im, push_re, push_im), axis=0)


def read_out(total_re, total_im, inputs, c_re, c_im, d_skip):
    length = inputs.shape[0]
    groups, channels, states = c_re.shape
    state_re = total_re.reshape(length, groups, states)
    state_im = total_im.reshape(length, groups, states)
    mixed = jnp.einsum("tgp,gnp->tgn", state_re, c_re, precision=HIGHEST)
    mixed = mixed - jnp.einsum("tgp,gnp->tgn", state_im, c_im, precision=HIGHEST)
    skipped = mixed.reshape(length, groups * channels) + d_skip * inputs.astype(jnp.float32)
    return jax.nn.gelu(skipped).astype(jnp.bfloat16)


def local(
    mix_in,
    mix_gain,
    lam_re,
    lam_im,
    log_dt,
    b_re,
    b_im,
    c_re,
    c_im,
    d_skip,
    log_retain,
    w_lin,
    w_glu,
    moe_in,
    moe_gain,
    routes,
    route_weight,
    w_gate,
    w_up,
    w_down,
):
    normed = root_mean_normed(mix_in, mix_gain)
    channels_here = d_skip.shape[0]
    own_inputs = lax.dynamic_slice_in_dim(
        normed, lax.axis_index("tp") * channels_here, channels_here, 1
    )
    log_mag, angle, drive_re, drive_im = discretize(lam_re, lam_im, log_dt, b_re, b_im)
    pref_re, pref_im, local_re, local_im = local_scan(
        own_inputs, log_retain, log_mag, angle, drive_re, drive_im
    )
    unity = jnp.ones_like(pref_re[-1])
    nought = jnp.zeros_like(pref_re[-1])
    incoming = prefix(
        (pref_re[-1], pref_im[-1], local_re[-1], local_im[-1]),
        "ep",
        compose,
        (unity, nought, nought, nought),
    )
    carry_re = incoming[2]
    carry_im = incoming[3]
    total_re = local_re + pref_re * carry_re - pref_im * carry_im
    total_im = local_im + pref_re * carry_im + pref_im * carry_re
    activated = read_out(total_re, total_im, own_inputs, c_re, c_im, d_skip)
    piece = lax.all_gather(activated, "tp", axis=1, tiled=True)
    mix_lin = jnp.dot(piece, w_lin, preferred_element_type=jnp.float32)
    mix_glu = jnp.dot(piece, w_glu, preferred_element_type=jnp.float32)
    mix_out = (mix_lin * jax.nn.sigmoid(mix_glu)).astype(jnp.bfloat16)
    normed_b = root_mean_normed(moe_in, moe_gain)
    experts = lax.axis_size("ep")
    tokens_here, choices_each = routes.shape
    capacity = 3 * choices_each * tokens_here // (2 * experts)
    flat_routes = routes.reshape(-1)
    onehot = (flat_routes[:, None] == jnp.arange(experts, dtype=jnp.int32)[None, :]).astype(
        jnp.int32
    )
    earlier_count = jnp.cumsum(onehot, axis=0) - onehot
    slot_index = jnp.sum(earlier_count * onehot, axis=1)
    target = flat_routes * capacity + slot_index
    places = jnp.arange(experts * capacity, dtype=jnp.int32)
    picked = jnp.any(
        places[:, None, None] == target.reshape(tokens_here, choices_each)[None], axis=2
    )
    picked = picked.astype(jnp.bfloat16)
    feature_slice = moe_in.shape[1] // lax.axis_size("tp")
    source_rows = lax.dynamic_slice_in_dim(
        normed_b, lax.axis_index("tp") * feature_slice, feature_slice, 1
    )
    outgoing = jnp.dot(picked, source_rows, preferred_element_type=jnp.float32).astype(jnp.bfloat16)
    outgoing = outgoing.reshape(experts, capacity, source_rows.shape[1])
    gate_local = w_gate[0]
    up_local = w_up[0]
    down_local = w_down[0]
    received = lax.all_to_all(outgoing, "ep", split_axis=0, concat_axis=0, tiled=True)
    senders, slots_here, features_here = received.shape
    piece = lax.all_gather(received, "tp", axis=2, tiled=True)
    piece_rows = piece.reshape(senders * slots_here, piece.shape[2])
    gate_pre = jnp.dot(piece_rows, gate_local, preferred_element_type=jnp.float32)
    up_pre = jnp.dot(piece_rows, up_local, preferred_element_type=jnp.float32)
    hidden = (jax.nn.silu(gate_pre) * up_pre).astype(jnp.bfloat16)
    partial_out = jnp.dot(hidden, down_local, preferred_element_type=jnp.float32).astype(
        jnp.bfloat16
    )
    partial_out = lax.optimization_barrier(partial_out)
    summed = lax.psum_scatter(
        partial_out.astype(jnp.float32).astype(jnp.bfloat16), "tp", scatter_dimension=1, tiled=True
    ).astype(jnp.float32)
    final_result = summed.astype(jnp.bfloat16).reshape(senders, slots_here, summed.shape[1])
    returned = lax.all_to_all(final_result, "ep", split_axis=0, concat_axis=0, tiled=True)
    flat_returned = returned.reshape(experts * capacity, returned.shape[2])
    gathered = (
        flat_returned[target]
        .astype(jnp.float32)
        .reshape(tokens_here, choices_each, returned.shape[2])
    )
    moe_out = jnp.sum(gathered * route_weight[:, :, None], axis=1).astype(jnp.bfloat16)
    return (mix_out, moe_out)


def solution(mesh):
    placed = (
        P("ep", None),
        P(),
        P("tp", None),
        P("tp", None),
        P("tp"),
        P("tp", None, None),
        P("tp", None, None),
        P("tp", None, None),
        P("tp", None, None),
        P("tp"),
        P("ep", "tp"),
        P(None, "tp"),
        P(None, "tp"),
        P("ep", None),
        P(),
        P("ep", None),
        P("ep", None),
        P("ep", None, "tp"),
        P("ep", None, "tp"),
        P("ep", "tp", None),
    )
    return jax.shard_map(
        local, mesh=mesh, in_specs=placed, out_specs=(P("ep", "tp"), P("ep", "tp")), check_vma=False
    )
```

profile of v0, /device:TPU:0, one launch (start us, length us, event | category | flops | bytes accessed | tf_op | source)
XLA Modules:
  0.0 1557.1 jit_solution(5644460298926567442)
XLA Ops:
  27.3 20.5 %slice.428 = f32[64,2048]{0,1:T(8,128)} slice(f32[128,2048]{0,1:T(8,128)S(1)} %bitcast.119), slice={[0:127:2], [0:2048:1]} | slice | bytes 1048576 | tf_op jit(solution)/shard_map/slice | solution.py:69
  47.7 21.9 %slice.431 = f32[64,2048]{0,1:T(8,128)} slice(f32[128,2048]{0,1:T(8,128)S(1)} %bitcast.120), slice={[1:128:2], [0:2048:1]} | slice | bytes 1048576 | tf_op jit(solution)/shard_map/slice | solution.py:69
  72.7 21.0 %slice.430 = f32[64,2048]{0,1:T(8,128)} slice(f32[128,2048]{0,1:T(8,128)} %bitcast.123), slice={[0:127:2], [0:2048:1]} | slice | bytes 1048576 | tf_op jit(solution)/shard_map/slice | solution.py:69
  93.7 21.9 %slice.439 = f32[64,2048]{0,1:T(8,128)} slice(f32[128,2048]{0,1:T(8,128)S(1)} %bitcast.125), slice={[1:128:2], [0:2048:1]} | slice | bytes 1048576 | tf_op jit(solution)/shard_map/slice | solution.py:69
  117.6 21.9 %slice.427 = f32[64,2048]{0,1:T(8,128)} slice(f32[128,2048]{0,1:T(8,128)S(1)} %get-tuple-element.312), slice={[1:128:2], [0:2048:1]} | slice | bytes 1048576 | tf_op jit(solution)/shard_map/slice | solution.py:69
  139.5 20.3 %slice.433 = f32[64,2048]{0,1:T(8,128)} slice(f32[128,2048]{0,1:T(8,128)S(1)} %get-tuple-element.312), slice={[0:127:2], [0:2048:1]} | slice | bytes 1048576 | tf_op jit(solution)/shard_map/slice | solution.py:69
  159.8 21.5 %slice.429 = f32[64,2048]{0,1:T(8,128)} slice(f32[128,2048]{0,1:T(8,128)} %get-tuple-element.313), slice={[1:128:2], [0:2048:1]} | slice | bytes 1048576 | tf_op jit(solution)/shard_map/slice | solution.py:69
  181.2 20.3 %slice.434 = f32[64,2048]{0,1:T(8,128)} slice(f32[128,2048]{0,1:T(8,128)S(1)} %copy-done.4), slice={[0:127:2], [0:2048:1]} | slice | bytes 1048576 | tf_op jit(solution)/shard_map/slice | solution.py:69
  206.9 11.5 slice.437
  218.5 11.8 slice.441
  230.2 11.1 slice.436
  241.3 10.8 slice.443
  252.2 11.8 slice.438
  264.0 10.8 slice.444
  274.9 11.5 slice.440
  286.4 11.1 slice.449
  302.9 8.5 slice.447
  311.4 8.6 slice.451
  333.3 8.7 slice.448
  348.4 8.5 slice.450
  376.1 7.3 slice.461
  393.5 7.4 slice.458
  594.3 8.4 slice.508
  602.7 8.5 slice.512
  611.2 8.4 slice.516
  619.6 10.8 slice.435
  630.4 11.5 slice.514
  641.9 10.8 slice.518
  652.8 11.5 slice.522
  664.2 21.0 %slice.524 = f32[63,2048]{0,1:T(8,128)} slice(f32[128,2048]{0,1:T(8,128)} %bitcast.121), slice={[2:128:2], [0:2048:1]} | slice | bytes 1032192 | tf_op jit(solution)/shard_map/slice | solution.py:69
  685.2 21.1 %slice.556 = f32[63,2048]{0,1:T(8,128)} slice(f32[128,2048]{0,1:T(8,128)} %bitcast.124), slice={[2:128:2], [0:2048:1]} | slice | bytes 1032192 | tf_op jit(solution)/shard_map/slice | solution.py:69
  706.3 21.6 %slice.426 = f32[63,2048]{0,1:T(8,128)} slice(f32[128,2048]{0,1:T(8,128)S(1)} %copy-done.3), slice={[2:128:2], [0:2048:1]} | slice | bytes 1032192 | tf_op jit(solution)/shard_map/slice | solution.py:69
  727.9 20.9 %slice.520 = f32[63,2048]{0,1:T(8,128)} slice(f32[128,2048]{0,1:T(8,128)} %get-tuple-element.313), slice={[2:128:2], [0:2048:1]} | slice | bytes 1032192 | tf_op jit(solution)/shard_map/slice | solution.py:69
  969.5 8.9 pad.190
  978.4 9.1 pad.191
  987.5 9.2 pad.189
  999.6 8.9 pad.188
  1018.0 13.3 pad.194
  1031.3 13.4 pad.195
  1047.5 13.2 pad.192
  1060.7 13.4 pad.193
  1129.2 22.4 %pad.227 = f32[128,2048]{0,1:T(8,128)} pad(f32[64,2048]{0,1:T(8,128)} %add.561, f32[]{:T(128)} %constant.55.clone.1), padding=1_0_1x0_0_0 | pad | bytes 1572868 | tf_op jit(solution)/shard_map/pad | solution.py:69
  1151.6 22.2 %pad.226 = f32[128,2048]{0,1:T(8,128)} pad(f32[64,2048]{0,1:T(8,128)} %pad_maximum_fusion.11, f32[]{:T(128)} %constant.55.clone.1), padding=0_1_1x0_0_0 | pad | bytes 1572868 | tf_op jit(solution)/shard_map/pad | solution.py:69
  1173.8 8.9 pad.216
  1182.7 9.2 pad.217
  1192.0 8.9 pad.214
  1200.9 9.1 pad.215
  1222.1 14.5 all-gather.3
  1236.6 22.3 %pad.197 = f32[128,2048]{0,1:T(8,128)} pad(f32[64,2048]{0,1:T(8,128)} %add.558, f32[]{:T(128)} %constant.55.clone.1), padding=1_0_1x0_0_0 | pad | bytes 1572868 | tf_op jit(solution)/shard_map/pad | solution.py:69
  1258.8 22.1 %pad.196 = f32[128,2048]{0,1:T(8,128)} pad(f32[64,2048]{0,1:T(8,128)} %pad_maximum_fusion.4, f32[]{:T(128)} %constant.55.clone.1), padding=0_1_1x0_0_0 | pad | bytes 1572868 | tf_op jit(solution)/shard_map/pad | solution.py:69
  1283.5 14.0 all-gather.2
  1298.8 13.2 pad.220
  1312.1 13.4 pad.221
  1325.5 13.4 pad.219
  1341.8 13.2 pad.218
  1362.6 22.0 %pad.224 = f32[128,2048]{0,1:T(8,128)} pad(f32[64,2048]{0,1:T(8,128)} %pad_maximum_fusion.10, f32[]{:T(128)} %constant.55.clone.1), padding=0_1_1x0_0_0 | pad | bytes 1572868 | tf_op jit(solution)/shard_map/pad | solution.py:69
  1384.6 22.4 %pad.225 = f32[128,2048]{0,1:T(8,128)} pad(f32[64,2048]{0,1:T(8,128)} %add.581, f32[]{:T(128)} %constant.55.clone.1), padding=1_0_1x0_0_0 | pad | bytes 1572868 | tf_op jit(solution)/shard_map/pad | solution.py:69
  1409.6 14.0 all-gather.1
  1425.0 19.5 %pad.222 = f32[128,2048]{0,1:T(8,128)S(1)} pad(f32[64,2048]{0,1:T(8,128)} %pad_maximum_fusion.9, f32[]{:T(128)} %constant.55.clone.1), padding=0_1_1x0_0_0 | pad | bytes 1572868 | tf_op jit(solution)/shard_map/pad | solution.py:69
  1444.5 22.4 %pad.223 = f32[128,2048]{0,1:T(8,128)} pad(f32[64,2048]{0,1:T(8,128)} %add.579, f32[]{:T(128)} %constant.55.clone.1), padding=1_0_1x0_0_0 | pad | bytes 1572868 | tf_op jit(solution)/shard_map/pad | solution.py:69
  1469.0 14.0 all-gather
  1488.6 9.1 fusion.6
  1506.1 23.8 %reduce-scatter.2.cloned.1.call-done = bf16[384,512]{1,0:T(8,128)(2,1)} async-done(((bf16[384,2048]{1,0:T(8,128)(2,1)}), bf16[384,512]{1,0:T(8,128)(2,1)}) %reduce-scatter.2.cloned.1.call-update) | async-done | bytes 393232 | tf_op jit(solution)/shard_map/reduce_scatter | solution.py:167
  1534.5 10.9 all_gather.22
  (511 shorter events, 624.9 us)
Async XLA Ops:
  7.2 1538.3 %copy-start = (bf16[2048,512]{1,0:T(8,128)(2,1)S(1)}, bf16[2048,512]{1,0:T(8,128)(2,1)}, u32[]{:S(2)}) copy-start(bf16[2048,512]{1,0:T(8,128)(2,1)} %param.33) | copy-start | bytes 6291460
  7.2 3.4 copy-start.94
  8.3 14.2 copy-start.95
  14.0 9.9 copy-start.116
  14.0 9.9 copy-start.107
  14.0 9.9 copy-start.108
  14.0 11.3 copy-start.96
  16.1 1198.3 %all-to-all-start = ((bf16[8,48,512]{2,1,0:T(8,128)(2,1)}), bf16[8,48,512]{2,1,0:T(8,128)(2,1)}, u32[]{:S(2)}, u32[]{:S(2)}) async-start(bf16[8,48,512]{2,1,0:T(8,128)(2,1)} %bitcast.16), calls=%async_computation | async-start | bytes 786432 | tf_op jit(solution)/shard_map/all_to_all | solution.py:156
  22.5 1460.5 %all-gather.6.cloned.1.call-start = ((), (), s32[]{:S(2)}) async-start(), calls=%async_computation.3 | async-start | bytes 1966080 | tf_op jit(solution)/shard_map/all_gather | solution.py:158
  27.3 42.4 %copy-start.10 = (f32[32,64,128]{2,1,0:T(8,128)}, f32[32,64,128]{2,1,0:T(8,128)S(1)}, u32[]{:S(2)}) copy-start(f32[32,64,128]{2,1,0:T(8,128)S(1)} %fusion.55) | copy-start | bytes 3145732
  72.7 21.0 %copy-start.12 = (f32[32,64,128]{2,1,0:T(8,128)S(1)}, f32[32,64,128]{2,1,0:T(8,128)}, u32[]{:S(2)}) copy-start(f32[32,64,128]{2,1,0:T(8,128)} %fusion.51) | copy-start | bytes 3145732
  72.7 42.9 %copy-start.103 = (f32[32,64]{1,0:T(8,128)S(1)}, f32[32,64]{1,0:T(8,128)}, u32[]{:S(2)}) copy-start(f32[32,64]{1,0:T(8,128)} %get-tuple-element.318) | copy-start | bytes 24580
  72.7 43.0 %copy-start.102 = (f32[32,64]{1,0:T(8,128)S(1)}, f32[32,64]{1,0:T(8,128)}, u32[]{:S(2)}) copy-start(f32[32,64]{1,0:T(8,128)} %get-tuple-element.314) | copy-start | bytes 24580
  72.7 43.0 %copy-start.101 = (f32[32,64]{1,0:T(8,128)S(1)}, f32[32,64]{1,0:T(8,128)}, u32[]{:S(2)}) copy-start(f32[32,64]{1,0:T(8,128)} %get-tuple-element.315) | copy-start | bytes 24580
  72.7 43.1 %copy-start.106 = (f32[128,32]{0,1:T(8,128)S(1)}, f32[128,32]{0,1:T(8,128)}, u32[]{:S(2)}) copy-start(f32[128,32]{0,1:T(8,128)} %param.32) | copy-start | bytes 49156
  117.6 42.2 %copy-start.2 = (f32[128,2048]{0,1:T(8,128)}, f32[128,2048]{0,1:T(8,128)S(1)}, u32[]{:S(2)}) copy-start(f32[128,2048]{0,1:T(8,128)S(1)} %get-tuple-element.312) | copy-start | bytes 3145732
  159.8 21.5 %copy-start.4 = (f32[128,2048]{0,1:T(8,128)S(1)}, f32[128,2048]{0,1:T(8,128)}, u32[]{:S(2)}) copy-start(f32[128,2048]{0,1:T(8,128)} %get-tuple-element.313) | copy-start | bytes 3145732
  206.9 34.4 %copy-start.6 = (f32[64,2048]{0,1:T(8,128)}, f32[64,2048]{0,1:T(8,128)S(1)}, u32[]{:S(2)}) copy-start(f32[64,2048]{0,1:T(8,128)S(1)} %get-tuple-element.229) | copy-start | bytes 1572868
  252.2 11.8 copy-start.8
  274.9 11.5 copy-start.20
  302.9 23.6 %copy-start.14 = (f32[32,2048]{0,1:T(8,128)}, f32[32,2048]{0,1:T(8,128)S(1)}, u32[]{:S(2)}) copy-start(f32[32,2048]{0,1:T(8,128)S(1)} %get-tuple-element.298) | copy-start | bytes 786436
  333.3 8.7 copy-start.17
  348.4 8.5 copy-start.25
  368.8 19.7 %copy-start.22 = (f32[16,2048]{0,1:T(8,128)}, f32[16,2048]{0,1:T(8,128)S(1)}, u32[]{:S(2)}) copy-start(f32[16,2048]{0,1:T(8,128)S(1)} %get-tuple-element.221) | copy-start | bytes 393220
  393.5 7.4 copy-start.24
  405.8 7.3 copy-start.27
  423.6 8.8 copy-start.28
  432.5 6.8 copy-start.31
  443.6 13.4 copy-start.29
  517.7 3.3 copy-start.87
  517.7 3.3 copy-start.88
  517.7 3.3 copy-start.89
  517.7 3.3 copy-start.90
  527.2 4.4 copy-start.32
  537.1 6.7 copy-start.30
  548.1 13.3 copy-start.23
  573.5 14.4 copy-start.15
  602.7 16.9 %copy-start.7 = (f32[64,2048]{0,1:T(8,128)S(1)}, f32[64,2048]{0,1:T(8,128)}, u32[]{:S(2)}) copy-start(f32[64,2048]{0,1:T(8,128)} %copy-done.6) | copy-start | bytes 1572868
  630.4 11.6 copy-start.19
  664.2 42.1 %copy-start.3 = (f32[128,2048]{0,1:T(8,128)S(1)}, f32[128,2048]{0,1:T(8,128)}, u32[]{:S(2)}) copy-start(f32[128,2048]{0,1:T(8,128)} %copy-done.2) | copy-start | bytes 3145732
  822.9 3.0 copy-start.86
  904.6 2.8 copy-start.48
  904.6 2.8 copy-start.54
  909.3 3.0 copy-start.84
  959.8 2.8 copy-start.58
  959.8 2.8 copy-start.59
  959.8 3.9 copy-start.81
  964.9 3.3 copy-start.26
  1008.4 3.9 copy-start.78
  1013.4 3.3 copy-start.21
  1113.6 4.0 copy-start.13
  1113.6 6.7 copy-start.82
  1214.5 315.4 %reduce-scatter.2.cloned.1.call-start = ((), (), s32[]{:S(2)}) async-start(), calls=%async_computation.4 | async-start | bytes 1966080 | tf_op jit(solution)/shard_map/reduce_scatter | solution.py:167
  1280.9 16.6 %copy-start.9 = (f32[64,2048]{0,1:T(8,128)S(1)}, f32[64,2048]{0,1:T(8,128)}, u32[]{:S(2)}) copy-start(f32[64,2048]{0,1:T(8,128)} %get-tuple-element.230) | copy-start | bytes 1572868
  1280.9 16.6 %copy-start.91 = (f32[31,2048]{0,1:T(8,128)S(1)}, f32[31,2048]{0,1:T(8,128)}, u32[]{:S(2)}) copy-start(f32[31,2048]{0,1:T(8,128)} %get-tuple-element.197) | copy-start | bytes 761860
  1354.9 2.8 copy-start.73
  1354.9 2.8 copy-start.74
  1354.9 3.9 copy-start.76
  1407.1 16.6 %copy-start.92 = (f32[63,2048]{0,1:T(8,128)S(1)}, f32[63,2048]{0,1:T(8,128)}, u32[]{:S(2)}) copy-start(f32[63,2048]{0,1:T(8,128)} %get-tuple-element.196) | copy-start | bytes 1548292
  1444.5 24.5 %copy-start.62 = (f32[128,2048]{0,1:T(8,128)}, f32[128,2048]{0,1:T(8,128)S(1)}, u32[]{:S(2)}) copy-start(f32[128,2048]{0,1:T(8,128)S(1)} %pad.222) | copy-start | bytes 3145732
  1498.9 3.6 copy-start.99
  1498.9 4.6 copy-start.97
  1529.9 17.2 %all-to-all-start.1 = ((bf16[8,48,512]{2,1,0:T(8,128)(2,1)}), bf16[8,48,512]{2,1,0:T(8,128)(2,1)S(1)}, u32[]{:S(2)}, u32[]{:S(2)}) async-start(bf16[8,48,512]{2,1,0:T(8,128)(2,1)} %bitcast.157), calls=%async_computation.2 | async-start | bytes 786432 | tf_op jit(solution)/shard_map/all_to_all | solution.py:171
  1534.5 11.4 copy-start.115
  (57 other events, 109.4 us)
Sparse Core Ops, SparseCore 0:
  1214.6 32.1 all-gather.5
  1497.8 32.0 reduce-scatter.1
where the time goes:
time: 1570 us; the launch traced here: 1560 us
  local copies, waits for them, and re-layouts  1270 us (81%)
  other arithmetic  141 us (9%)
  blocking collectives  67.3 us (4%)
  matrix products  25.4 us (2%)
  waiting for transfers between devices  23.8 us (2%)
    slice x69, local copies, waits for them, and re-layouts, local_scan(): lax.associative_scan(compose, (decay_re, decay_im, push_re, push_im), axi...  673 us
    pad x48, local copies, waits for them, and re-layouts, local_scan(): lax.associative_scan(compose, (decay_re, decay_im, push_re, push_im), axi...  497 us
    all_gather x4, blocking collectives, prefix(): pieces = jax.tree.map(lambda part: lax.all_gather(part, axis), value)  56.4 us
    unnamed x258, local copies, waits for them, and re-layouts  44.5 us
    add x22, other arithmetic, local_scan(): lax.associative_scan(compose, (decay_re, decay_im, push_re, push_im), axi...  34.5 us
  transfers between devices with their start and end apart: 4, of which 1 were waited for; matrix products, arithmetic and copies ran while one was open for 90% of the time, Pallas kernels for 0%

commit v1 on v0

v1 whole, which is shorter than its diff:
```python
import functools

import jax
import jax.numpy as jnp
from jax import lax
from jax.experimental import pallas as pl
from jax.experimental.pallas import tpu as pltpu
from jax.sharding import PartitionSpec as P

EPS = 1e-06


def root_mean_normed(values, gain):
    broadened_rows = values.astype(jnp.float32)
    inverse = lax.rsqrt(jnp.mean(broadened_rows * broadened_rows, axis=-1, keepdims=True) + EPS)
    return (broadened_rows * inverse * gain).astype(jnp.bfloat16)


def discretize(lam_re, lam_im, log_dt):
    time_step = jnp.exp(log_dt)[:, None]
    log_mag = lam_re * time_step
    angle = lam_im * time_step
    half_sine = jnp.sin(0.5 * angle)
    minus_re = jnp.expm1(log_mag) * jnp.cos(angle) - 2.0 * half_sine * half_sine
    minus_im = jnp.exp(log_mag) * jnp.sin(angle)
    denom = lam_re * lam_re + lam_im * lam_im
    coef_re = (minus_re * lam_re + minus_im * lam_im) / denom
    coef_im = (minus_im * lam_re - minus_re * lam_im) / denom
    magnitude = jnp.exp(log_mag)
    return coef_re, coef_im, magnitude * jnp.cos(angle), magnitude * jnp.sin(angle)


CHUNKS = 8
LANES = 128
MESH = pl.DeviceIdType.MESH


def split(value, terms):
    parts = []
    for _ in range(terms):
        part = value.astype(jnp.bfloat16)
        parts.append(part)
        value = value - part.astype(jnp.float32)
    return parts


def cmul(a_re, a_im, b_re, b_im):
    return a_re * b_re - a_im * b_im, a_re * b_im + a_im * b_re


def cpow(re, im, power):
    out = None
    while power:
        if power & 1:
            out = (re, im) if out is None else cmul(*out, re, im)
        power >>= 1
        if power:
            re, im = cmul(re, im, re, im)
    return out


def mixer_kernel(
    n_ep, n_tp, sizes, u_ref, keep_ref, coef_ref, mats_ref, skip_ref, out_ref,
    mag, push_re, push_im, ends, first, packed, gath, send_sem, recv_sem, tp_send, tp_recv,
):
    length, groups, states, channels = sizes
    width = groups * states
    steps = length // CHUNKS
    span_groups = LANES // channels
    span = span_groups * states
    spans = groups // span_groups
    rows = width // LANES
    per_span = span // LANES
    me, mine = lax.axis_index("ep"), lax.axis_index("tp")

    barrier = pltpu.get_barrier_semaphore()
    for d in range(1, n_ep):
        pl.semaphore_signal(
            barrier, inc=1, device_id=(lax.rem(me + d, n_ep), mine), device_id_type=MESH
        )
    for d in range(1, n_tp):
        pl.semaphore_signal(
            barrier, inc=1, device_id=(me, lax.rem(mine + d, n_tp)), device_id_type=MESH
        )

    def dot(x, y, dims=((1,), (0,))):
        return lax.dot_general(x, y, (dims, ((), ())), preferred_element_type=jnp.float32)

    row = lax.broadcasted_iota(jnp.int32, (length, length), 0)
    col = lax.broadcasted_iota(jnp.int32, (length, length), 1)
    order = ((row & (CHUNKS - 1)) * steps + (row >> 3) == col).astype(jnp.bfloat16)
    back = ((col & (CHUNKS - 1)) * steps + (col >> 3) == row).astype(jnp.bfloat16)
    u = dot(order, u_ref[...]).astype(jnp.bfloat16)
    keeps = [
        dot(order, part).astype(jnp.bfloat16) for part in split(jnp.exp(keep_ref[...]), 3)
    ]
    row = lax.broadcasted_iota(jnp.int32, (LANES, span), 0)
    col = lax.broadcasted_iota(jnp.int32, (LANES, span), 1)
    same = jnp.zeros((LANES, span), jnp.bool_)
    for g in range(span_groups):
        same = same | (
            (row >= g * channels) & (row < (g + 1) * channels)
            & (col >= g * states) & (col < (g + 1) * states)
        )

    def spread(value):
        return jnp.where(same, jnp.concatenate([value] * span_groups, axis=0), 0.0)

    for s in range(spans):
        at = slice(s * span, (s + 1) * span)
        group = lax.broadcasted_iota(jnp.int32, (groups, span), 0)
        lane = lax.broadcasted_iota(jnp.int32, (groups, span), 1) + s * span
        chosen = ((lane >= group * states) & (lane < (group + 1) * states)).astype(jnp.bfloat16)
        mag[:, at] = sum(dot(part, chosen) for part in keeps)
        b_re, b_im = mats_ref[0, :, at], mats_ref[1, :, at]
        co_re, co_im = coef_ref[0:1, at], coef_ref[1:2, at]
        own = u[:, s * LANES : (s + 1) * LANES]
        drive_re, drive_im = cmul(co_re, co_im, b_re, b_im)
        push_re[:, at] = sum(dot(own, part) for part in split(spread(drive_re), 2))
        push_im[:, at] = sum(dot(own, part) for part in split(spread(drive_im), 2))

    for s in range(spans):
        at = slice(s * span, (s + 1) * span)
        w_re = jnp.broadcast_to(coef_ref[2:3, at], (CHUNKS, span))
        w_im = jnp.broadcast_to(coef_ref[3:4, at], (CHUNKS, span))

        def turn(j, state, at=at, w_re=w_re, w_im=w_im):
            re, im, total = state
            here = pl.ds(pl.multiple_of(j * CHUNKS, CHUNKS), CHUNKS)
            m = mag[here, at]
            d_re, d_im = m * w_re, m * w_im
            re, im = cmul(d_re, d_im, re, im)
            return re + push_re[here, at], im + push_im[here, at], total * m

        zero = jnp.zeros((CHUNKS, span), jnp.float32)
        re, im, total = lax.fori_loop(0, steps, turn, (zero, zero, zero + 1.0))
        p_re, p_im = cpow(w_re, w_im, steps)
        ends[0, :, at] = re
        ends[1, :, at] = im
        ends[2, :, at] = total * p_re
        ends[3, :, at] = total * p_im
        ends[4, :, at] = total

    def chain(s, re, im, keep_all):
        at = slice(s * span, (s + 1) * span)
        for k in range(CHUNKS):
            if keep_all:
                first[0, k : k + 1, at] = re
                first[1, k : k + 1, at] = im
            if k < CHUNKS - 1 or not keep_all:
                re, im = cmul(ends[2, k : k + 1, at], ends[3, k : k + 1, at], re, im)
                re = re + ends[0, k : k + 1, at]
                im = im + ends[1, k : k + 1, at]
        return re, im

    for s in range(spans):
        at = slice(s * span, (s + 1) * span)
        zero = jnp.zeros((1, span), jnp.float32)
        re, im = chain(s, zero, zero, False)
        total = ends[4, 0:1, at]
        for k in range(1, CHUNKS):
            total = total * ends[4, k : k + 1, at]
        w_re, w_im = cpow(coef_ref[2:3, at], coef_ref[3:4, at], length)
        for i in range(per_span):
            r, cut = s * per_span + i, slice(i * LANES, (i + 1) * LANES)
            gath[me, r : r + 1, :] = re[:, cut]
            gath[me, rows + r : rows + r + 1, :] = im[:, cut]
            gath[me, 2 * rows + r : 2 * rows + r + 1, :] = total[:, cut]
            packed[r : r + 1, :] = w_re[:, cut]
            packed[rows + r : rows + r + 1, :] = w_im[:, cut]

    pl.semaphore_wait(barrier, n_ep - 1 + n_tp - 1)
    copies = []
    for d in range(1, n_ep):
        copy = pltpu.make_async_remote_copy(
            src_ref=gath.at[me], dst_ref=gath.at[me],
            send_sem=send_sem.at[d - 1], recv_sem=recv_sem.at[d - 1],
            device_id=(lax.rem(me + d, n_ep), mine), device_id_type=MESH,
        )
        copy.start()
        copies.append(copy)
    for copy in copies:
        copy.wait()
    wl_re, wl_im = packed[0:rows, :], packed[rows : 2 * rows, :]

    def join(i, state):
        re, im = state
        total = gath[i, 2 * rows : 3 * rows, :]
        n_re, n_im = cmul(total * wl_re, total * wl_im, re, im)
        n_re = n_re + gath[i, 0:rows, :]
        n_im = n_im + gath[i, rows : 2 * rows, :]
        return jnp.where(i < me, n_re, re), jnp.where(i < me, n_im, im)

    zero = jnp.zeros((rows, LANES), jnp.float32)
    in_re, in_im = lax.fori_loop(0, n_ep - 1, join, (zero, zero))
    packed[0:rows, :] = in_re
    packed[rows : 2 * rows, :] = in_im

    for s in range(spans):
        at = slice(s * span, (s + 1) * span)
        lines = range(s * per_span, (s + 1) * per_span)
        re = jnp.concatenate([packed[r : r + 1, :] for r in lines], axis=1)
        im = jnp.concatenate([packed[rows + r : rows + r + 1, :] for r in lines], axis=1)
        chain(s, re, im, True)
        w_re = jnp.broadcast_to(coef_ref[2:3, at], (CHUNKS, span))
        w_im = jnp.broadcast_to(coef_ref[3:4, at], (CHUNKS, span))

        def again(j, state, at=at, w_re=w_re, w_im=w_im):
            re, im = state
            here = pl.ds(pl.multiple_of(j * CHUNKS, CHUNKS), CHUNKS)
            m = mag[here, at]
            re, im = cmul(m * w_re, m * w_im, re, im)
            re, im = re + push_re[here, at], im + push_im[here, at]
            push_re[here, at] = re
            push_im[here, at] = im
            return re, im

        lax.fori_loop(0, steps, again, (first[0, :, at], first[1, :, at]))

    for s in range(spans):
        at = slice(s * span, (s + 1) * span)
        cut = slice(s * LANES, (s + 1) * LANES)
        mixed = jnp.zeros((length, LANES), jnp.float32)
        for ref, which, sign in ((push_re, 2, 1.0), (push_im, 3, -1.0)):
            x_hi, x_lo = split(ref[:, at], 2)
            c_hi, c_lo = split(spread(mats_ref[which, :, at]) * sign, 2)
            across = ((1,), (1,))
            mixed = mixed + dot(x_hi, c_hi, across)
            mixed = mixed + dot(x_hi, c_lo, across) + dot(x_lo, c_hi, across)
        x = mixed + skip_ref[:, cut] * u[:, cut].astype(jnp.float32)
        inner = 0.7978845608028654 * (x + 0.044715 * (x * x * x))
        act = (0.5 * x * (1.0 + jnp.tanh(inner))).astype(jnp.bfloat16)
        start = pl.multiple_of(mine * (spans * LANES) + s * LANES, LANES)
        out_ref[:, pl.ds(start, LANES)] = dot(back, act).astype(jnp.bfloat16)

    block = pl.ds(pl.multiple_of(mine * (spans * LANES), LANES), spans * LANES)
    copies = []
    for d in range(1, n_tp):
        copy = pltpu.make_async_remote_copy(
            src_ref=out_ref.at[:, block], dst_ref=out_ref.at[:, block],
            send_sem=tp_send.at[d - 1], recv_sem=tp_recv.at[d - 1],
            device_id=(me, lax.rem(mine + d, n_tp)), device_id_type=MESH,
        )
        copy.start()
        copies.append(copy)
    for copy in copies:
        copy.wait()


def mixer(inputs, retain, lam_re, lam_im, log_dt, b_re, b_im, c_re, c_im, d_skip):
    length, here = inputs.shape
    groups, channels, states = c_re.shape
    width = groups * states
    n_ep, n_tp = lax.axis_size("ep"), lax.axis_size("tp")
    coef = jnp.stack(discretize(lam_re, lam_im, log_dt)).reshape(4, width)
    mats = jnp.stack(
        [
            jnp.transpose(b_re, (2, 0, 1)),
            jnp.transpose(b_im, (2, 0, 1)),
            jnp.transpose(c_re, (1, 0, 2)),
            jnp.transpose(c_im, (1, 0, 2)),
        ]
    ).reshape(4, channels, width)
    rows = width // LANES
    big = pltpu.VMEM((length, width), jnp.float32)
    dma = pltpu.SemaphoreType.DMA
    return pl.pallas_call(
        functools.partial(mixer_kernel, n_ep, n_tp, (length, groups, states, channels)),
        out_shape=jax.ShapeDtypeStruct((length, here * n_tp), jnp.bfloat16),
        in_specs=[pl.BlockSpec(memory_space=pltpu.VMEM)] * 5,
        out_specs=pl.BlockSpec(memory_space=pltpu.VMEM),
        scratch_shapes=[
            big, big, big,
            pltpu.VMEM((5, CHUNKS, width), jnp.float32),
            pltpu.VMEM((2, CHUNKS, width), jnp.float32),
            pltpu.VMEM((2 * rows, LANES), jnp.float32),
            pltpu.VMEM((n_ep, 3 * rows, LANES), jnp.float32),
            dma((n_ep - 1,)), dma((n_ep - 1,)), dma((n_tp - 1,)), dma((n_tp - 1,)),
        ],
        compiler_params=pltpu.CompilerParams(collective_id=0, has_side_effects=True),
        cost_estimate=pl.CostEstimate(
            flops=20_000_000_000, bytes_accessed=4_000_000, transcendentals=0
        ),
    )(inputs, retain, coef, mats, d_skip.reshape(1, here))


def local(
    mix_in,
    mix_gain,
    lam_re,
    lam_im,
    log_dt,
    b_re,
    b_im,
    c_re,
    c_im,
    d_skip,
    log_retain,
    w_lin,
    w_glu,
    moe_in,
    moe_gain,
    routes,
    route_weight,
    w_gate,
    w_up,
    w_down,
):
    normed = root_mean_normed(mix_in, mix_gain)
    channels_here = d_skip.shape[0]
    own_inputs = lax.dynamic_slice_in_dim(
        normed, lax.axis_index("tp") * channels_here, channels_here, 1
    )
    piece = mixer(
        own_inputs, log_retain, lam_re, lam_im, log_dt, b_re, b_im, c_re, c_im, d_skip
    )
    mix_lin = jnp.dot(piece, w_lin, preferred_element_type=jnp.float32)
    mix_glu = jnp.dot(piece, w_glu, preferred_element_type=jnp.float32)
    mix_out = (mix_lin * jax.nn.sigmoid(mix_glu)).astype(jnp.bfloat16)
    normed_b = root_mean_normed(moe_in, moe_gain)
    experts = lax.axis_size("ep")
    tokens_here, choices_each = routes.shape
    capacity = 3 * choices_each * tokens_here // (2 * experts)
    flat_routes = routes.reshape(-1)
    onehot = (flat_routes[:, None] == jnp.arange(experts, dtype=jnp.int32)[None, :]).astype(
        jnp.int32
    )
    earlier_count = jnp.cumsum(onehot, axis=0) - onehot
    slot_index = jnp.sum(earlier_count * onehot, axis=1)
    target = flat_routes * capacity + slot_index
    places = jnp.arange(experts * capacity, dtype=jnp.int32)
    picked = jnp.any(
        places[:, None, None] == target.reshape(tokens_here, choices_each)[None], axis=2
    )
    picked = picked.astype(jnp.bfloat16)
    feature_slice = moe_in.shape[1] // lax.axis_size("tp")
    source_rows = lax.dynamic_slice_in_dim(
        normed_b, lax.axis_index("tp") * feature_slice, feature_slice, 1
    )
    outgoing = jnp.dot(picked, source_rows, preferred_element_type=jnp.float32).astype(jnp.bfloat16)
    outgoing = outgoing.reshape(experts, capacity, source_rows.shape[1])
    gate_local = w_gate[0]
    up_local = w_up[0]
    down_local = w_down[0]
    received = lax.all_to_all(outgoing, "ep", split_axis=0, concat_axis=0, tiled=True)
    senders, slots_here, features_here = received.shape
    piece = lax.all_gather(received, "tp", axis=2, tiled=True)
    piece_rows = piece.reshape(senders * slots_here, piece.shape[2])
    gate_pre = jnp.dot(piece_rows, gate_local, preferred_element_type=jnp.float32)
    up_pre = jnp.dot(piece_rows, up_local, preferred_element_type=jnp.float32)
    hidden = (jax.nn.silu(gate_pre) * up_pre).astype(jnp.bfloat16)
    partial_out = jnp.dot(hidden, down_local, preferred_element_type=jnp.float32).astype(
        jnp.bfloat16
    )
    partial_out = lax.optimization_barrier(partial_out)
    summed = lax.psum_scatter(
        partial_out.astype(jnp.float32).astype(jnp.bfloat16), "tp", scatter_dimension=1, tiled=True
    ).astype(jnp.float32)
    final_result = summed.astype(jnp.bfloat16).reshape(senders, slots_here, summed.shape[1])
    returned = lax.all_to_all(final_result, "ep", split_axis=0, concat_axis=0, tiled=True)
    flat_returned = returned.reshape(experts * capacity, returned.shape[2])
    gathered = (
        flat_returned[target]
        .astype(jnp.float32)
        .reshape(tokens_here, choices_each, returned.shape[2])
    )
    moe_out = jnp.sum(gathered * route_weight[:, :, None], axis=1).astype(jnp.bfloat16)
    return (mix_out, moe_out)


def solution(mesh):
    placed = (
        P("ep", None),
        P(),
        P("tp", None),
        P("tp", None),
        P("tp"),
        P("tp", None, None),
        P("tp", None, None),
        P("tp", None, None),
        P("tp", None, None),
        P("tp"),
        P("ep", "tp"),
        P(None, "tp"),
        P(None, "tp"),
        P("ep", None),
        P(),
        P("ep", None),
        P("ep", None),
        P("ep", None, "tp"),
        P("ep", None, "tp"),
        P("ep", "tp", None),
    )
    return jax.shard_map(
        local, mesh=mesh, in_specs=placed, out_specs=(P("ep", "tp"), P("ep", "tp")), check_vma=False
    )
```

time: 1570 us -> 138 us (0.09)
  local copies, waits for them, and re-layouts: 1270 us -> 8.83 us
  other arithmetic: 141 us -> 9.26 us
  blocking collectives: 67.3 us -> 18.9 us
  Pallas kernels: 0 us -> 21.1 us
  waiting for transfers between devices: 23.8 us -> 42.1 us
    slice x70 -> x1, local copies, waits for them, and re-layouts: 673 us -> 0.21 us  [the longest x69 673 us: local_scan(): lax.associative_scan(compose, (decay_re, decay_im, push_re, push_im), axi...]
    pad x48 -> x0, local copies, waits for them, and re-layouts: 497 us -> none  [local_scan(): lax.associative_scan(compose, (decay_re, decay_im, push_re, push_im), axi...]
    add x42 -> x0, other arithmetic: 69.7 us -> none  [the longest x22 34.5 us: local_scan(): lax.associative_scan(compose, (decay_re, decay_im, push_re, push_im), axi...]
    all_gather x5 -> x0, blocking collectives: 67.3 us -> none  [the longest x4 56.4 us: prefix(): pieces = jax.tree.map(lambda part: lax.all_gather(part, axis), value)]
    unnamed x258 -> x27, local copies, waits for them, and re-layouts: 44.5 us -> 1.94 us
    mul x26 -> x0, local copies, waits for them, and re-layouts: 37.5 us -> none  [the longest x3 4.69 us: compose(): late_im * shift_im]
    all_gather x1, waiting for transfers between devices: 0.02 us -> 23.5 us  [local(): piece = lax.all_gather(received, 'tp', axis=2, tiled=True)]
    pallas_call x0 -> x1, Pallas kernels: none -> 21.1 us  [mixer(): pl.pallas_call(functools.partial(mixer_kernel, n_ep, n_tp, (length, group...]
  transfers between devices with their start and end apart: 4 -> 3, of which waited for: 1 -> 3; matrix products, arithmetic and copies ran while one was open for 90% -> 9% of each run, Pallas kernels for 0% -> 15%
where the time goes in v1:
time: 138 us
  waiting for transfers between devices  42.1 us (31%)
  Pallas kernels  21.1 us (15%)
  blocking collectives  18.9 us (14%)
  matrix products  18.7 us (14%)
  between operations  14.3 us (10%)
  other arithmetic  9.26 us (7%)
  local copies, waits for them, and re-layouts  8.83 us (6%)
  starting transfers between devices  4.69 us (3%)
    all_gather x1, waiting for transfers between devices, local(): piece = lax.all_gather(received, 'tp', axis=2, tiled=True)  23.5 us
    pallas_call x1, Pallas kernels, mixer(): pl.pallas_call(functools.partial(mixer_kernel, n_ep, n_tp, (length, group...  21.1 us
    all_to_all x1, blocking collectives, local(): lax.all_to_all(outgoing, 'ep', split_axis=0, concat_axis=0, tiled=True)  18.9 us
    all_to_all x1, waiting for transfers between devices, local(): lax.all_to_all(final_result, 'ep', split_axis=0, concat_axis=0, tiled=True)  9.61 us
    dot_general x1, matrix products, local(): jnp.dot(hidden, down_local, preferred_element_type=jnp.float32)  9.04 us
    reduce_scatter x1, waiting for transfers between devices, local(): lax.psum_scatter(partial_out.astype(jnp.float32).astype(jnp.bfloat16), 't...  8.91 us
    dot_general x1, matrix products, local(): jnp.dot(piece_rows, gate_local, preferred_element_type=jnp.float32)  5.59 us
    all_to_all x1, starting transfers between devices, local(): lax.all_to_all(final_result, 'ep', split_axis=0, concat_axis=0, tiled=True)  4.61 us
  transfers between devices with their start and end apart: 3, of which 3 were waited for; matrix products, arithmetic and copies ran while one was open for 9% of the time, Pallas kernels for 15%

profile of v1, /device:TPU:0, one launch (start us, length us, event | category | flops | bytes accessed | tf_op | source)
XLA Modules:
  0.0 137.9 jit_solution(2062477927245162795)
XLA Ops:
  7.2 0.0 copy-start
  7.2 0.0 copy-start.1
  7.2 0.0 all-gather.2.cloned.1.call-start
  7.2 1.0 copy.43
  8.2 0.1 eq.43
  8.3 0.1 eq.39
  8.5 0.0 copy-start.9
  8.5 0.0 copy-start.2
  8.5 2.2 %convert_element_type.51 = f32[128,2048]{1,0:T(8,128)} convert(bf16[128,2048]{1,0:T(8,128)(2,1)} %param.33) | non-fusion elementwise | flops 262144 | bytes 1572864 | tf_op jit(solution)/shard_map/convert_element_type | solution.py:14
  10.7 0.2 multiply_reduce_fusion
  10.9 0.0 copy-start.7
  10.9 0.0 copy-start.8
  10.9 0.6 reduce-window.6
  11.5 0.2 slice_reduce_fusion
  11.8 0.1 fusion.31
  11.9 0.1 reduce_sum.42
  12.0 0.0 copy-start.4
  12.1 0.1 copy.46
  12.1 0.1 fusion.19
  12.2 0.8 dynamic-slice.1
  13.0 1.3 convolution_convert_fusion
  14.3 0.0 copy-start.5
  14.3 18.9 %all_to_all.10 = bf16[8,48,512]{2,1,0:T(8,128)(2,1)} all-to-all(bf16[8,48,512]{2,1,0:T(8,128)(2,1)S(1)} %bitcast.42), channel_id=1, replica_groups=mesh['ep'=8,'tp'=4] {'ep'}, dimensions={0} | all-to-all | bytes 786432 | tf_op jit(solution)/shard_map/all_to_all | solution.py:345
  33.2 0.0 all-gather.2.cloned.1.call-update
  33.2 0.0 reduce-scatter.2.cloned.1.call-start
  33.3 0.1 mul.172
  33.4 0.1 copy.47
  33.5 0.8 dynamic-slice
  34.3 1.1 convert_element_type.46
  35.4 0.0 copy-done.11
  35.4 0.2 fusion.28
  35.7 0.1 stack.30
  35.7 0.1 stack.31
  35.8 0.1 stack.32
  35.9 0.1 stack.33
  36.0 0.1 copy.38
  36.1 0.1 stack.35
  36.2 0.0 copy-done.5
  36.2 0.1 copy.39
  36.3 0.1 stack.36
  36.4 1.0 copy.40
  37.5 0.1 stack.37
  37.6 1.0 copy.41
  38.6 0.1 stack.38
  38.7 0.7 copy.42.keep_ref
  39.5 23.5 %all-gather.2.cloned.1.call-done = bf16[8,48,2048]{2,1,0:T(8,128)(2,1)} async-done(((bf16[8,48,512]{2,1,0:T(8,128)(2,1)}), bf16[8,48,2048]{2,1,0:T(8,128)(2,1)}) %all-gather.2.cloned.1.call-update) | async-done | bytes 1572880 | tf_op jit(solution)/shard_map/all_gather | solution.py:347
  63.0 5.6 %fusion.4 = f32[384,1024]{1,0:T(8,128)} fusion(bf16[384,2048]{1,0:T(8,128)(2,1)} %bitcast.50, bf16[1,2048,1024]{2,1,0:T(8,128)(2,1)} %param.37), kind=kOutput, calls=%fused_computation.5 | convolution fusion | flops 1610612736 | bytes 7340032 | tf_op jit(solution)/shard_map/dot_general | solution.py:349
  68.6 9.0 %fusion.6 = bf16[384,2048]{1,0:T(8,128)(2,1)} fusion(bf16[1,1024,2048]{2,1,0:T(8,128)(2,1)} %param.39, f32[384,1024]{1,0:T(8,128)} %fusion.4, bf16[384,2048]{1,0:T(8,128)(2,1)} %bitcast.51, bf16[1,2048,1024]{2,1,0:T(8,128)(2,1)} %param.38), kind=kOutput, calls=%fused_computation.7 | convolution fusion | flops 3224371200 | bytes 13107200 | tf_op jit(solution)/shard_map/dot_general | solution.py:352
  77.6 0.0 reduce-scatter.2.cloned.1.call-update
  77.7 0.2 multiply_reduce_fusion.1
  77.9 0.6 pad_maximum_fusion.1.coef_ref
  78.5 1.7 %fusion.23.u_ref = bf16[128,512]{1,0:T(8,128)(2,1)} fusion(f32[128,2048]{1,0:T(8,128)} %convert_element_type.46, s32[]{:T(128)S(6)} %select_n.14, f32[512]{0:T(512)S(1)} %dynamic-slice, f32[128]{0:T(128)S(1)} %add_rsqrt_fusion.1), kind=kLoop, calls=%fused_computation.28 | loop fusion | flops 196608 | bytes 395780 | tf_op jit(solution)/shard_map/convert_element_type | solution.py:16
  80.2 0.8 pad_maximum_fusion.mats_ref
  81.0 21.1 %shard_map.203 = bf16[128,2048]{1,0:T(8,128)(2,1)} custom-call(bf16[128,512]{1,0:T(8,128)(2,1)} %fusion.23.u_ref, f32[128,32]{1,0:T(8,128)} %copy.42.keep_ref, f32[4,2048]{1,0:T(4,128)} %pad_maximum_fusion.1.coef_ref, f32[4,16,2048]{2,1,0:T(8,128)} %pad_maximum_fusion.mats_ref, f32[1,512]{1,0:T(1,128)} %bitcast.52), custom_call_target="tpu_custom_call" | custom-call | flops 20000000000 | bytes 4000000 | tf_op jit(solution)/shard_map/pallas_call | solution.py:267
  102.1 8.9 %reduce-scatter.2.cloned.1.call-done = bf16[384,512]{1,0:T(8,128)(2,1)} async-done(((bf16[384,2048]{1,0:T(8,128)(2,1)}), bf16[384,512]{1,0:T(8,128)(2,1)}) %reduce-scatter.2.cloned.1.call-update) | async-done | bytes 393232 | tf_op jit(solution)/shard_map/reduce_scatter | solution.py:356
  111.1 4.6 %all-to-all-start.1 = ((bf16[8,48,512]{2,1,0:T(8,128)(2,1)}), bf16[8,48,512]{2,1,0:T(8,128)(2,1)S(1)}, u32[]{:S(2)}, u32[]{:S(2)}) async-start(bf16[8,48,512]{2,1,0:T(8,128)(2,1)} %bitcast.43), calls=%async_computation.2 | async-start | bytes 786432 | tf_op jit(solution)/shard_map/all_to_all | solution.py:360
  115.7 1.6 %fusion.36 = f32[128,512]{1,0:T(8,128)S(1)} fusion(bf16[128,2048]{1,0:T(8,128)(2,1)} %shard_map.203, bf16[2048,512]{1,0:T(8,128)(2,1)S(1)} %copy-done), kind=kOutput, calls=%fused_computation.56 | convolution fusion | flops 268435456 | bytes 2883584 | tf_op jit(solution)/shard_map/dot_general | solution.py:317
  117.3 0.0 copy-done.3
  117.3 0.1 copy-done.10
  117.4 1.2 fusion.15
  118.6 9.6 %all-to-all-done.1 = bf16[8,48,512]{2,1,0:T(8,128)(2,1)S(1)} async-done(((bf16[8,48,512]{2,1,0:T(8,128)(2,1)}), bf16[8,48,512]{2,1,0:T(8,128)(2,1)S(1)}, u32[]{:S(2)}, u32[]{:S(2)}) %all-to-all-start.1) | async-done | bytes 393248 | tf_op jit(solution)/shard_map/all_to_all | solution.py:360
  128.2 1.2 gather_fusion
  129.3 0.3 reshape.119
  129.7 1.4 multiply_reduce_fusion.2
  (21 shorter events, 0.1 us)
Async XLA Ops:
  7.2 108.5 %copy-start = (bf16[2048,512]{1,0:T(8,128)(2,1)S(1)}, bf16[2048,512]{1,0:T(8,128)(2,1)}, u32[]{:S(2)}) copy-start(bf16[2048,512]{1,0:T(8,128)(2,1)} %param.31) | copy-start | bytes 6291460
  7.2 3.5 %copy-start.1 = (bf16[128,2048]{1,0:T(8,128)(2,1)S(1)}, bf16[128,2048]{1,0:T(8,128)(2,1)}, u32[]{:S(2)}) copy-start(bf16[128,2048]{1,0:T(8,128)(2,1)} %param.33) | copy-start | bytes 1572868
  7.2 55.8 %all-gather.2.cloned.1.call-start = ((), (), s32[]{:S(2)}) async-start(), calls=%async_computation.3 | async-start | bytes 1966080 | tf_op jit(solution)/shard_map/all_gather | solution.py:347
  8.5 24.9 %copy-start.9 = (f32[128,2]{0,1:T(2,128)S(1)}, f32[128,2]{0,1:T(2,128)}, u32[]{:S(2)}) copy-start(f32[128,2]{0,1:T(2,128)} %param.36) | copy-start | bytes 3076
  8.5 25.8 %copy-start.2 = (bf16[128,2048]{1,0:T(8,128)(2,1)S(1)}, bf16[128,2048]{1,0:T(8,128)(2,1)}, u32[]{:S(2)}) copy-start(bf16[128,2048]{1,0:T(8,128)(2,1)} %param.20) | copy-start | bytes 1572868
  10.9 24.5 %copy-start.11 = (f32[32]{0:T(128)S(1)}, f32[32]{0:T(128)}, u32[]{:S(2)}) copy-start(f32[32]{0:T(128)} %param.24) | copy-start | bytes 388
  10.9 24.5 %copy-start.7 = (f32[32,64]{1,0:T(8,128)S(1)}, f32[32,64]{1,0:T(8,128)}, u32[]{:S(2)}) copy-start(f32[32,64]{1,0:T(8,128)} %param.23) | copy-start | bytes 24580
  10.9 24.5 %copy-start.8 = (f32[32,64]{1,0:T(8,128)S(1)}, f32[32,64]{1,0:T(8,128)}, u32[]{:S(2)}) copy-start(f32[32,64]{1,0:T(8,128)} %param.22) | copy-start | bytes 24580
  12.0 24.0 %copy-start.4 = (f32[32,64,16]{1,2,0:T(8,128)S(1)}, f32[32,64,16]{1,2,0:T(8,128)}, u32[]{:S(2)}) copy-start(f32[32,64,16]{1,2,0:T(8,128)} %param.25) | copy-start | bytes 393220
  14.3 21.9 %copy-start.5 = (f32[32,64,16]{1,2,0:T(8,128)S(1)}, f32[32,64,16]{1,2,0:T(8,128)}, u32[]{:S(2)}) copy-start(f32[32,64,16]{1,2,0:T(8,128)} %param.26) | copy-start | bytes 393220
  33.2 77.8 %reduce-scatter.2.cloned.1.call-start = ((), (), s32[]{:S(2)}) async-start(), calls=%async_computation.4 | async-start | bytes 1966080 | tf_op jit(solution)/shard_map/reduce_scatter | solution.py:356
  35.4 3.3 %copy-start.6 = (f32[128,32]{0,1:T(8,128)S(1)}, f32[128,32]{0,1:T(8,128)}, u32[]{:S(2)}) copy-start(f32[128,32]{0,1:T(8,128)} %param.30) | copy-start | bytes 49156
  102.1 15.2 %copy-start.3 = (bf16[128,2048]{1,0:T(8,128)(2,1)S(1)}, bf16[128,2048]{1,0:T(8,128)(2,1)}, u32[]{:S(2)}) copy-start(bf16[128,2048]{1,0:T(8,128)(2,1)} %shard_map.203) | copy-start | bytes 1572868
  111.1 17.1 %all-to-all-start.1 = ((bf16[8,48,512]{2,1,0:T(8,128)(2,1)}), bf16[8,48,512]{2,1,0:T(8,128)(2,1)S(1)}, u32[]{:S(2)}, u32[]{:S(2)}) async-start(bf16[8,48,512]{2,1,0:T(8,128)(2,1)} %bitcast.43), calls=%async_computation.2 | async-start | bytes 786432 | tf_op jit(solution)/shard_map/all_to_all | solution.py:360
  115.7 1.7 %copy-start.10 = (bf16[2048,512]{1,0:T(8,128)(2,1)S(1)}, bf16[2048,512]{1,0:T(8,128)(2,1)}, u32[]{:S(2)}) copy-start(bf16[2048,512]{1,0:T(8,128)(2,1)} %param.32) | copy-start | bytes 6291460
Sparse Core Ops, SparseCore 0:
  33.3 29.6 all-gather.1
  77.8 33.2 reduce-scatter.1

commit v2 on v1

--- a/solution.py
+++ b/solution.py
@@ -60,8 +60,9 @@
 
 
 def mixer_kernel(
-    n_ep, n_tp, sizes, u_ref, keep_ref, coef_ref, mats_ref, skip_ref, out_ref,
+    n_ep, n_tp, sizes, u_ref, keep_ref, coef_ref, mats_ref, skip_ref, rows_ref, out_ref, got_ref,
     mag, push_re, push_im, ends, first, packed, gath, send_sem, recv_sem, tp_send, tp_recv,
+    route_send, route_recv, share_send, share_recv,
 ):
     length, groups, states, channels = sizes
     width = groups * states
@@ -82,6 +83,42 @@
         pl.semaphore_signal(
             barrier, inc=1, device_id=(me, lax.rem(mine + d, n_tp)), device_id_type=MESH
         )
+
+    features = rows_ref.shape[2]
+    columns = pl.ds(pl.multiple_of(mine * features, LANES), features)
+
+    def route(d):
+        return pltpu.make_async_remote_copy(
+            src_ref=rows_ref.at[lax.rem(me + d, n_ep)], dst_ref=got_ref.at[me, :, columns],
+            send_sem=route_send.at[d - 1], recv_sem=route_recv.at[d - 1],
+            device_id=(lax.rem(me + d, n_ep), mine), device_id_type=MESH,
+        )
+
+    def share(d, hop, source=None):
+        sender = lax.rem(me + n_ep - d, n_ep)
+        block = got_ref.at[sender, :, columns]
+        return pltpu.make_async_remote_copy(
+            src_ref=block if source is None else source, dst_ref=block,
+            send_sem=share_send.at[d, hop - 1], recv_sem=share_recv.at[d, hop - 1],
+            device_id=(me, lax.rem(mine + hop, n_tp)), device_id_type=MESH,
+        )
+
+    def forward(low, high):
+        @pl.loop(low, high)
+        def _(d):
+            route(d).wait_recv()
+            for hop in range(1, n_tp):
+                share(d, hop).start()
+
+    pl.semaphore_wait(barrier, n_ep - 1 + n_tp - 1)
+
+    @pl.loop(1, n_ep)
+    def _(d):
+        route(d).start()
+
+    for hop in range(1, n_tp):
+        share(0, hop, rows_ref.at[me]).start()
+    got_ref[me, :, columns] = rows_ref[me]
 
     def dot(x, y, dims=((1,), (0,))):
         return lax.dot_general(x, y, (dims, ((), ())), preferred_element_type=jnp.float32)
@@ -118,6 +155,7 @@
         drive_re, drive_im = cmul(co_re, co_im, b_re, b_im)
         push_re[:, at] = sum(dot(own, part) for part in split(spread(drive_re), 2))
         push_im[:, at] = sum(dot(own, part) for part in split(spread(drive_im), 2))
+        forward(1 + (n_ep - 1) * s // (2 * spans), 1 + (n_ep - 1) * (s + 1) // (2 * spans))
 
     for s in range(spans):
         at = slice(s * span, (s + 1) * span)
@@ -169,7 +207,6 @@
             packed[r : r + 1, :] = w_re[:, cut]
             packed[rows + r : rows + r + 1, :] = w_im[:, cut]
 
-    pl.semaphore_wait(barrier, n_ep - 1 + n_tp - 1)
     copies = []
     for d in range(1, n_ep):
         copy = pltpu.make_async_remote_copy(
@@ -179,6 +216,7 @@
         )
         copy.start()
         copies.append(copy)
+    forward(1 + (n_ep - 1) // 2, n_ep)
     for copy in copies:
         copy.wait()
     wl_re, wl_im = packed[0:rows, :], packed[rows : 2 * rows, :]
@@ -245,9 +283,104 @@
         copies.append(copy)
     for copy in copies:
         copy.wait()
-
-
-def mixer(inputs, retain, lam_re, lam_im, log_dt, b_re, b_im, c_re, c_im, d_skip):
+    for hop in range(1, n_tp):
+        share(0, hop, rows_ref.at[me]).wait()
+
+    @pl.loop(1, n_ep)
+    def _(d):
+        route(d).wait_send()
+        for hop in range(1, n_tp):
+            share(d, hop).wait()
+
+
+def return_kernel(n_ep, n_tp, part_ref, out_ref, parts, summed, tp_send, tp_recv, send, recv):
+    me, mine = lax.axis_index("ep"), lax.axis_index("tp")
+    features = out_ref.shape[2]
+    barrier = pltpu.get_barrier_semaphore()
+    for d in range(1, n_ep):
+        pl.semaphore_signal(
+            barrier, inc=1, device_id=(lax.rem(me + d, n_ep), mine), device_id_type=MESH
+        )
+    for d in range(1, n_tp):
+        pl.semaphore_signal(
+            barrier, inc=1, device_id=(me, lax.rem(mine + d, n_tp)), device_id_type=MESH
+        )
+    pl.semaphore_wait(barrier, n_ep - 1 + n_tp - 1)
+
+    def columns(index):
+        return pl.ds(pl.multiple_of(index * features, LANES), features)
+
+    def scatter(d, hop):
+        owner, peer = lax.rem(me + d, n_ep), lax.rem(mine + hop, n_tp)
+        return pltpu.make_async_remote_copy(
+            src_ref=part_ref.at[owner, :, columns(peer)], dst_ref=parts.at[owner, hop - 1],
+            send_sem=tp_send.at[d - 1, hop - 1], recv_sem=tp_recv.at[d - 1, hop - 1],
+            device_id=(me, peer), device_id_type=MESH,
+        )
+
+    def home(d):
+        owner = lax.rem(me + d, n_ep)
+        return pltpu.make_async_remote_copy(
+            src_ref=summed.at[owner], dst_ref=out_ref.at[me],
+            send_sem=send.at[d - 1], recv_sem=recv.at[d - 1],
+            device_id=(owner, mine), device_id_type=MESH,
+        )
+
+    def total(d):
+        owner = lax.rem(me + d, n_ep)
+        value = part_ref[owner, :, columns(mine)].astype(jnp.float32)
+        for hop in range(1, n_tp):
+            scatter(d, hop).wait_recv()
+            value = value + parts[owner, hop - 1].astype(jnp.float32)
+        return owner, value.astype(jnp.bfloat16)
+
+    @pl.loop(1, n_ep + 1)
+    def _(d):
+        for hop in range(1, n_tp):
+            scatter(d, hop).start()
+
+    @pl.loop(1, n_ep)
+    def _(d):
+        owner, value = total(d)
+        summed[owner] = value
+        home(d).start()
+
+    _, value = total(n_ep)
+    out_ref[me] = value
+
+    @pl.loop(1, n_ep)
+    def _(d):
+        home(d).wait()
+
+    @pl.loop(1, n_ep + 1)
+    def _(d):
+        for hop in range(1, n_tp):
+            scatter(d, hop).wait_send()
+
+
+def give_back(partial_out):
+    n_ep, n_tp = lax.axis_size("ep"), lax.axis_size("tp")
+    _, slots, width = partial_out.shape
+    features = width // n_tp
+    dma = pltpu.SemaphoreType.DMA
+    return pl.pallas_call(
+        functools.partial(return_kernel, n_ep, n_tp),
+        out_shape=jax.ShapeDtypeStruct((n_ep, slots, features), jnp.bfloat16),
+        in_specs=[pl.BlockSpec(memory_space=pltpu.VMEM)],
+        out_specs=pl.BlockSpec(memory_space=pltpu.VMEM),
+        scratch_shapes=[
+            pltpu.VMEM((n_ep, n_tp - 1, slots, features), jnp.bfloat16),
+            pltpu.VMEM((n_ep, slots, features), jnp.bfloat16),
+            dma((n_ep, n_tp - 1)), dma((n_ep, n_tp - 1)), dma((n_ep - 1,)), dma((n_ep - 1,)),
+        ],
+        compiler_params=pltpu.CompilerParams(collective_id=1, has_side_effects=True),
+        cost_estimate=pl.CostEstimate(
+            flops=20_000_000_000, bytes_accessed=4_000_000, transcendentals=0
+        ),
+    )(partial_out)
+
+
+def mixer(inputs, retain, lam_re, lam_im, log_dt, b_re, b_im, c_re, c_im, d_skip, outgoing):
     length, here = inputs.shape
     groups, channels, states = c_re.shape
     width = groups * states
@@ -262,13 +395,17 @@
         ]
     ).reshape(4, channels, width)
     rows = width // LANES
+    _, slots, features = outgoing.shape
     big = pltpu.VMEM((length, width), jnp.float32)
     dma = pltpu.SemaphoreType.DMA
     return pl.pallas_call(
         functools.partial(mixer_kernel, n_ep, n_tp, (length, groups, states, channels)),
-        out_shape=jax.ShapeDtypeStruct((length, here * n_tp), jnp.bfloat16),
-        in_specs=[pl.BlockSpec(memory_space=pltpu.VMEM)] * 5,
-        out_specs=pl.BlockSpec(memory_space=pltpu.VMEM),
+        out_shape=(
+            jax.ShapeDtypeStruct((length, here * n_tp), jnp.bfloat16),
+            jax.ShapeDtypeStruct((n_ep, slots, features * n_tp), jnp.bfloat16),
+        ),
+        in_specs=[pl.BlockSpec(memory_space=pltpu.VMEM)] * 6,
+        out_specs=(pl.BlockSpec(memory_space=pltpu.VMEM),) * 2,
         scratch_shapes=[
             big, big, big,
             pltpu.VMEM((5, CHUNKS, width), jnp.float32),
@@ -276,12 +413,13 @@
             pltpu.VMEM((2 * rows, LANES), jnp.float32),
             pltpu.VMEM((n_ep, 3 * rows, LANES), jnp.float32),
             dma((n_ep - 1,)), dma((n_ep - 1,)), dma((n_tp - 1,)), dma((n_tp - 1,)),
+            dma((n_ep - 1,)), dma((n_ep - 1,)), dma((n_ep, n_tp - 1)), dma((n_ep, n_tp - 1)),
         ],
         compiler_params=pltpu.CompilerParams(collective_id=0, has_side_effects=True),
         cost_estimate=pl.CostEstimate(
             flops=20_000_000_000, bytes_accessed=4_000_000, transcendentals=0
         ),
-    )(inputs, retain, coef, mats, d_skip.reshape(1, here))
+    )(inputs, retain, coef, mats, d_skip.reshape(1, here), outgoing)
 
 
 def local(
@@ -311,12 +449,6 @@
     own_inputs = lax.dynamic_slice_in_dim(
         normed, lax.axis_index("tp") * channels_here, channels_here, 1
     )
-    piece = mixer(
-        own_inputs, log_retain, lam_re, lam_im, log_dt, b_re, b_im, c_re, c_im, d_skip
-    )
-    mix_lin = jnp.dot(piece, w_lin, preferred_element_type=jnp.float32)
-    mix_glu = jnp.dot(piece, w_glu, preferred_element_type=jnp.float32)
-    mix_out = (mix_lin * jax.nn.sigmoid(mix_glu)).astype(jnp.bfloat16)
     normed_b = root_mean_normed(moe_in, moe_gain)
     experts = lax.axis_size("ep")
     tokens_here, choices_each = routes.shape
@@ -342,22 +474,17 @@
     gate_local = w_gate[0]
     up_local = w_up[0]
     down_local = w_down[0]
-    received = lax.all_to_all(outgoing, "ep", split_axis=0, concat_axis=0, tiled=True)
-    senders, slots_here, features_here = received.shape
-    piece = lax.all_gather(received, "tp", axis=2, tiled=True)
-    piece_rows = piece.reshape(senders * slots_here, piece.shape[2])
+    piece, received = mixer(
+        own_inputs, log_retain, lam_re, lam_im, log_dt, b_re, b_im, c_re, c_im, d_skip, outgoing
+    )
+    piece_rows = received.reshape(experts * capacity, received.shape[2])
     gate_pre = jnp.dot(piece_rows, gate_local, preferred_element_type=jnp.float32)
     up_pre = jnp.dot(piece_rows, up_local, preferred_element_type=jnp.float32)
     hidden = (jax.nn.silu(gate_pre) * up_pre).astype(jnp.bfloat16)
     partial_out = jnp.dot(hidden, down_local, preferred_element_type=jnp.float32).astype(
         jnp.bfloat16
     )
-    partial_out = lax.optimization_barrier(partial_out)
-    summed = lax.psum_scatter(
-        partial_out.astype(jnp.float32).astype(jnp.bfloat16), "tp", scatter_dimension=1, tiled=True
-    ).astype(jnp.float32)
-    final_result = summed.astype(jnp.bfloat16).reshape(senders, slots_here, summed.shape[1])
-    returned = lax.all_to_all(final_result, "ep", split_axis=0, concat_axis=0, tiled=True)
+    returned = give_back(partial_out.reshape(experts, capacity, partial_out.shape[1]))
     flat_returned = returned.reshape(experts * capacity, returned.shape[2])
     gathered = (
         flat_returned[target]
@@ -365,6 +492,9 @@
         .reshape(tokens_here, choices_each, returned.shape[2])
     )
     moe_out = jnp.sum(gathered * route_weight[:, :, None], axis=1).astype(jnp.bfloat16)
+    mix_lin = jnp.dot(piece, w_lin, preferred_element_type=jnp.float32)
+    mix_glu = jnp.dot(piece, w_glu, preferred_element_type=jnp.float32)
+    mix_out = (mix_lin * jax.nn.sigmoid(mix_glu)).astype(jnp.bfloat16)
     return (mix_out, moe_out)
 
 

time: 138 us -> 95.7 us (0.69)
  waiting for transfers between devices: 42.1 us -> 0 us
  Pallas kernels: 21.1 us -> 60.2 us
  blocking collectives: 18.9 us -> 0 us
  between operations: 14.3 us -> 0.92 us
  starting transfers between devices: 4.69 us -> 0 us
  other arithmetic: 9.26 us -> 7.44 us
    pallas_call x0 -> x1, Pallas kernels: none -> 26.6 us  [give_back(): pl.pallas_call(functools.partial(return_kernel, n_ep, n_tp), out_shape=ja...]
    all_gather x1 -> x0, waiting for transfers between devices: 23.5 us -> none  [local(): piece = lax.all_gather(received, 'tp', axis=2, tiled=True)]
    all_to_all x1 -> x0, blocking collectives: 18.9 us -> none  [local(): lax.all_to_all(outgoing, 'ep', split_axis=0, concat_axis=0, tiled=True)]
    pallas_call x1, Pallas kernels: 21.1 us -> 33.6 us  [mixer(): pl.pallas_call(functools.partial(mixer_kernel, n_ep, n_tp, (length, group...]
    all_to_all x1 -> x0, waiting for transfers between devices: 9.61 us -> none  [local(): lax.all_to_all(final_result, 'ep', split_axis=0, concat_axis=0, tiled=True)]
    reduce_scatter x1 -> x0, waiting for transfers between devices: 8.91 us -> none  [local(): lax.psum_scatter(partial_out.astype(jnp.float32).astype(jnp.bfloat16), 't...]
    all_to_all x1 -> x0, starting transfers between devices: 4.61 us -> none  [local(): lax.all_to_all(final_result, 'ep', split_axis=0, concat_axis=0, tiled=True)]
    dot_general x1, matrix products: 5.59 us -> 2.95 us  [local(): jnp.dot(piece_rows, gate_local, preferred_element_type=jnp.float32)]
  transfers between devices with their start and end apart: 3 -> 0, of which waited for: 3 -> 0; matrix products, arithmetic and copies ran while one was open for 9% -> 0% of each run, Pallas kernels for 15% -> 0%
where the time goes in v2:
time: 95.7 us; the launch traced here: 95.2 us
  Pallas kernels  60.2 us (63%)
  matrix products  17.6 us (18%)
  local copies, waits for them, and re-layouts  9.02 us (9%)
  other arithmetic  7.44 us (8%)
    pallas_call x1, Pallas kernels, mixer(): pl.pallas_call(functools.partial(mixer_kernel, n_ep, n_tp, (length, group...  33.6 us
    pallas_call x1, Pallas kernels, give_back(): pl.pallas_call(functools.partial(return_kernel, n_ep, n_tp), out_shape=ja...  26.6 us
    dot_general x1, matrix products, local(): jnp.dot(hidden, down_local, preferred_element_type=jnp.float32)  9.03 us
    dot_general x1, matrix products, local(): jnp.dot(piece_rows, gate_local, preferred_element_type=jnp.float32)  2.95 us
    dot_general x1, matrix products, local(): mix_glu = jnp.dot(piece, w_glu, preferred_element_type=jnp.float32)  2.89 us
    gather x1, local copies, waits for them, and re-layouts, local(): flat_returned[target].astype(jnp.float32)  2.26 us

profile of v2, /device:TPU:0, one launch (start us, length us, event | category | flops | bytes accessed | tf_op | source)
XLA Modules:
  0.0 95.2 jit_solution(11444172205509435464)
XLA Ops:
  0.6 0.0 copy-start
  0.6 0.0 copy-start.5
  0.7 0.0 copy-start.6
  0.7 0.0 copy-start.7
  0.7 0.0 copy-start.11
  0.7 0.0 copy-start.3
  0.7 1.3 %convert_element_type.42 = f32[128,2048]{1,0:T(8,128)S(1)} convert(bf16[128,2048]{1,0:T(8,128)(2,1)} %param.20) | non-fusion elementwise | flops 262144 | bytes 1572864 | tf_op jit(solution)/shard_map/convert_element_type | solution.py:14
  2.0 0.8 dynamic-slice
  2.8 1.2 %multiply_reduce_fusion.1 = f32[128]{0:T(128)S(1)} fusion(bf16[128,2048]{1,0:T(8,128)(2,1)} %param.20), kind=kLoop, calls=%fused_computation.17 | loop fusion | flops 786304 | bytes 524800 | tf_op jit(solution)/shard_map/reduce_sum | solution.py:15
  4.0 0.8 fusion.23.u_ref
  4.8 0.0 copy-done.5
  4.8 0.7 copy.46.keep_ref
  5.5 0.0 copy-done.11
  5.5 0.0 copy-done.6
  5.5 0.0 copy-done.7
  5.5 0.2 fusion.28
  5.7 0.1 stack.33
  5.8 0.1 stack.32
  5.9 0.1 stack.31
  6.0 0.1 stack.30
  6.0 0.6 pad_maximum_fusion.1.coef_ref
  6.7 0.0 copy-done.3
  6.7 0.1 copy.41
  6.8 0.0 copy-start.8
  6.8 0.1 stack.38
  6.9 1.0 %copy.40 = f32[16,32,64]{2,1,0:T(8,128)S(1)} copy(f32[16,32,64]{2,0,1:T(8,128)} %bitcast.44) | data formatting | bytes 262144 | tf_op jit(solution)/shard_map/transpose | solution.py:393
  7.9 0.0 copy-start.1
  8.0 0.1 stack.37
  8.1 0.0 copy-done.4
  8.1 0.1 copy.39
  8.2 0.1 stack.36
  8.3 1.0 %copy.38 = f32[16,32,64]{2,1,0:T(8,128)S(1)} copy(f32[16,32,64]{2,0,1:T(8,128)} %bitcast.46) | data formatting | bytes 262144 | tf_op jit(solution)/shard_map/transpose | solution.py:391
  9.3 0.1 stack.35
  9.5 0.8 pad_maximum_fusion.mats_ref
  10.3 0.1 copy.42
  10.4 0.1 eq.43
  10.6 0.6 reduce-window.6
  11.2 0.2 slice_reduce_fusion
  11.4 0.1 eq.39
  11.6 0.1 fusion.31
  11.7 0.1 reduce_sum.42
  11.8 0.1 copy.45
  11.9 0.1 fusion.19
  12.0 0.1 convert_element_type.46
  12.1 0.8 dynamic-slice.1
  12.8 0.2 multiply_reduce_fusion
  13.0 1.1 %convolution_convert_fusion = bf16[384,512]{1,0:T(8,128)(2,1)} fusion(pred[384,128]{1,0:T(8,128)(4,1)S(1)} %fusion.19, f32[128,2048]{1,0:T(8,128)S(1)} %convert_element_type.46, s32[]{:T(128)S(6)} %select_n.14, f32[512]{0:T(512)S(1)} %dynamic-slice.1, f32[128]{0:T(128)S(1)} %add_rsqrt_fusion), kind=kOutput, calls=%fused_computation.9 | convolution fusion | flops 50724864 | bytes 707076 | tf_op jit(solution)/shard_map/dot_general | solution.py:472
  14.1 33.6 %shard_map.203 = (bf16[128,2048]{1,0:T(8,128)(2,1)}, bf16[8,48,2048]{2,1,0:T(8,128)(2,1)}) custom-call(bf16[128,512]{1,0:T(8,128)(2,1)} %fusion.23.u_ref, f32[128,32]{1,0:T(8,128)} %copy.46.keep_ref, f32[4,2048]{1,0:T(4,128)} %pad_maximum_fusion.1.coef_ref, f32[4,16,2048]{2,1,0:T(8,128)} %pad_maximum_fusion.mats_ref, f32[1,512]{1,0:T(1,128)} %bitcast.49, ...), custom_call_target="tpu_custom_call" | custom-call | flops 20000000000 | bytes 4000000 | tf_op jit(solution)/shard_map/pallas_call | solution.py:401
  47.8 0.0 copy-start.10
  47.8 1.6 %fusion.36 = f32[128,512]{1,0:T(8,128)S(1)} fusion(bf16[128,2048]{1,0:T(8,128)(2,1)} %get-tuple-element.4, bf16[2048,512]{1,0:T(8,128)(2,1)S(1)} %copy-done), kind=kOutput, calls=%fused_computation.56 | convolution fusion | flops 268435456 | bytes 2883584 | tf_op jit(solution)/shard_map/dot_general | solution.py:495
  49.4 0.0 copy-done.2
  49.4 0.0 copy-start.12
  49.5 2.9 %fusion.15 = bf16[128,512]{1,0:T(8,128)(2,1)} fusion(f32[128,512]{1,0:T(8,128)S(1)} %fusion.36, bf16[128,2048]{1,0:T(8,128)(2,1)S(1)} %copy-done.2, bf16[2048,512]{1,0:T(8,128)(2,1)} %param.32), kind=kOutput, calls=%fused_computation.15 | convolution fusion | flops 268763136 | bytes 3014656 | tf_op jit(solution)/shard_map/dot_general | solution.py:496
  52.3 0.0 copy-done.12
  52.4 2.9 %fusion.4 = f32[384,1024]{1,0:T(8,128)} fusion(bf16[384,2048]{1,0:T(8,128)(2,1)S(1)} %bitcast.51, bf16[1,2048,1024]{2,1,0:T(8,128)(2,1)S(1)} %copy-done.10), kind=kOutput, calls=%fused_computation.5 | convolution fusion | flops 1610612736 | bytes 7340032 | tf_op jit(solution)/shard_map/dot_general | solution.py:481
  55.3 9.0 %fusion.6 = bf16[384,2048]{1,0:T(8,128)(2,1)} fusion(bf16[1,1024,2048]{2,1,0:T(8,128)(2,1)} %param.39, f32[384,1024]{1,0:T(8,128)} %fusion.4, bf16[384,2048]{1,0:T(8,128)(2,1)} %bitcast.50, bf16[1,2048,1024]{2,1,0:T(8,128)(2,1)} %param.38), kind=kOutput, calls=%fused_computation.7 | convolution fusion | flops 3224371200 | bytes 13107200 | tf_op jit(solution)/shard_map/dot_general | solution.py:484
  64.3 26.6 %shard_map.204 = bf16[8,48,512]{2,1,0:T(8,128)(2,1)} custom-call(bf16[8,48,2048]{2,1,0:T(8,128)(2,1)} %bitcast.52), custom_call_target="tpu_custom_call" | custom-call | flops 20000000000 | bytes 4000000 | tf_op jit(solution)/shard_map/pallas_call | solution.py:366
  90.9 0.0 copy-start.9
  90.9 0.1 mul.172
  91.1 2.3 %gather_fusion = bf16[256,512]{1,0:T(8,128)(2,1)S(1)} fusion(bf16[384,512]{1,0:T(8,128)(2,1)} %bitcast.41, s32[1024]{0:T(1024)S(1)} %pad_clamp_fusion), kind=kCustom, calls=%fused_computation | custom fusion | bytes 525312 | tf_op jit(solution)/shard_map/gather | solution.py:490
  93.4 0.3 reshape.119
  93.7 0.0 copy-done.9
  93.7 0.1 copy.47
  93.8 1.4 %multiply_reduce_fusion.2 = bf16[128,512]{1,0:T(8,128)(2,1)} fusion(f32[128,2,512]{2,1,0:T(2,128)S(1)} %reshape.119, f32[128,2]{1,0:T(8,128)S(1)} %copy.47), kind=kLoop, calls=%fused_computation.20 | loop fusion | flops 196608 | bytes 656384 | tf_op jit(solution)/shard_map/reduce_sum | solution.py:494
  (15 shorter events, 0.1 us)
Async XLA Ops:
  0.6 47.1 %copy-start = (bf16[2048,512]{1,0:T(8,128)(2,1)S(1)}, bf16[2048,512]{1,0:T(8,128)(2,1)}, u32[]{:S(2)}) copy-start(bf16[2048,512]{1,0:T(8,128)(2,1)} %param.31) | copy-start | bytes 6291460
  0.6 4.1 %copy-start.5 = (f32[128,32]{0,1:T(8,128)S(1)}, f32[128,32]{0,1:T(8,128)}, u32[]{:S(2)}) copy-start(f32[128,32]{0,1:T(8,128)} %param.30) | copy-start | bytes 49156
  0.7 4.8 %copy-start.6 = (f32[32,64]{1,0:T(8,128)S(1)}, f32[32,64]{1,0:T(8,128)}, u32[]{:S(2)}) copy-start(f32[32,64]{1,0:T(8,128)} %param.23) | copy-start | bytes 24580
  0.7 4.8 %copy-start.7 = (f32[32,64]{1,0:T(8,128)S(1)}, f32[32,64]{1,0:T(8,128)}, u32[]{:S(2)}) copy-start(f32[32,64]{1,0:T(8,128)} %param.22) | copy-start | bytes 24580
  0.7 4.8 %copy-start.11 = (f32[32]{0:T(128)S(1)}, f32[32]{0:T(128)}, u32[]{:S(2)}) copy-start(f32[32]{0:T(128)} %param.24) | copy-start | bytes 388
  0.7 6.0 %copy-start.3 = (f32[32,16,64]{2,1,0:T(8,128)S(1)}, f32[32,16,64]{2,1,0:T(8,128)}, u32[]{:S(2)}) copy-start(f32[32,16,64]{2,1,0:T(8,128)} %param.28) | copy-start | bytes 393220
  4.8 3.3 %copy-start.4 = (f32[32,64,16]{1,2,0:T(8,128)S(1)}, f32[32,64,16]{1,2,0:T(8,128)}, u32[]{:S(2)}) copy-start(f32[32,64,16]{1,2,0:T(8,128)} %param.26) | copy-start | bytes 393220
  6.8 3.5 %copy-start.8 = (s32[128,2]{0,1:T(2,128)S(1)}, s32[128,2]{0,1:T(2,128)}, u32[]{:S(2)}) copy-start(s32[128,2]{0,1:T(2,128)} %param.35) | copy-start | bytes 3076
  7.9 4.0 %copy-start.1 = (bf16[128,2048]{1,0:T(8,128)(2,1)S(1)}, bf16[128,2048]{1,0:T(8,128)(2,1)}, u32[]{:S(2)}) copy-start(bf16[128,2048]{1,0:T(8,128)(2,1)} %param.33) | copy-start | bytes 1572868
  47.8 1.7 %copy-start.2 = (bf16[128,2048]{1,0:T(8,128)(2,1)S(1)}, bf16[128,2048]{1,0:T(8,128)(2,1)}, u32[]{:S(2)}) copy-start(bf16[128,2048]{1,0:T(8,128)(2,1)} %get-tuple-element.4) | copy-start | bytes 1572868
  47.8 4.6 %copy-start.10 = (bf16[1,2048,1024]{2,1,0:T(8,128)(2,1)S(1)}, bf16[1,2048,1024]{2,1,0:T(8,128)(2,1)}, u32[]{:S(2)}) copy-start(bf16[1,2048,1024]{2,1,0:T(8,128)(2,1)} %param.37) | copy-start | bytes 12582916
  49.4 2.9 %copy-start.12 = (bf16[8,48,2048]{2,1,0:T(8,128)(2,1)S(1)}, bf16[8,48,2048]{2,1,0:T(8,128)(2,1)}, u32[]{:S(2)}) copy-start(bf16[8,48,2048]{2,1,0:T(8,128)(2,1)} %get-tuple-element.5) | copy-start | bytes 4718596
  90.9 2.8 %copy-start.9 = (f32[128,2]{0,1:T(2,128)S(1)}, f32[128,2]{0,1:T(2,128)}, u32[]{:S(2)}) copy-start(f32[128,2]{0,1:T(2,128)} %param.36) | copy-start | bytes 3076

commit v3 on v1

--- a/solution.py
+++ b/solution.py
@@ -60,8 +60,9 @@
 
 
 def mixer_kernel(
-    n_ep, n_tp, sizes, u_ref, keep_ref, coef_ref, mats_ref, skip_ref, out_ref,
+    n_ep, n_tp, sizes, u_ref, keep_ref, coef_ref, mats_ref, skip_ref, part_ref, out_ref, home_ref,
     mag, push_re, push_im, ends, first, packed, gath, send_sem, recv_sem, tp_send, tp_recv,
+    route_send, route_recv, share_send, share_recv, parts, summed,
 ):
     length, groups, states, channels = sizes
     width = groups * states
@@ -82,6 +83,48 @@
         pl.semaphore_signal(
             barrier, inc=1, device_id=(me, lax.rem(mine + d, n_tp)), device_id_type=MESH
         )
+
+    features = home_ref.shape[2]
+    pl.semaphore_wait(barrier, n_ep - 1 + n_tp - 1)
+
+    def columns(index):
+        return pl.ds(pl.multiple_of(index * features, LANES), features)
+
+    def scatter(d, hop):
+        owner, peer = lax.rem(me + d, n_ep), lax.rem(mine + hop, n_tp)
+        return pltpu.make_async_remote_copy(
+            src_ref=part_ref.at[owner, :, columns(peer)], dst_ref=parts.at[owner, hop - 1],
+            send_sem=share_send.at[d - 1, hop - 1], recv_sem=share_recv.at[d - 1, hop - 1],
+            device_id=(me, peer), device_id_type=MESH,
+        )
+
+    def home(d):
+        owner = lax.rem(me + d, n_ep)
+        return pltpu.make_async_remote_copy(
+            src_ref=summed.at[owner], dst_ref=home_ref.at[me],
+            send_sem=route_send.at[d - 1], recv_sem=route_recv.at[d - 1],
+            device_id=(owner, mine), device_id_type=MESH,
+        )
+
+    def added(d):
+        owner = lax.rem(me + d, n_ep)
+        value = part_ref[owner, :, columns(mine)].astype(jnp.float32)
+        for hop in range(1, n_tp):
+            scatter(d, hop).wait_recv()
+            value = value + parts[owner, hop - 1].astype(jnp.float32)
+        return owner, value.astype(jnp.bfloat16)
+
+    @pl.loop(1, n_ep + 1)
+    def _(d):
+        for hop in range(1, n_tp):
+            scatter(d, hop).start()
+
+    def forward(low, high):
+        @pl.loop(low, high)
+        def _(d):
+            owner, value = added(d)
+            summed[owner] = value
+            home(d).start()
 
     def dot(x, y, dims=((1,), (0,))):
         return lax.dot_general(x, y, (dims, ((), ())), preferred_element_type=jnp.float32)
@@ -118,6 +161,7 @@
         drive_re, drive_im = cmul(co_re, co_im, b_re, b_im)
         push_re[:, at] = sum(dot(own, part) for part in split(spread(drive_re), 2))
         push_im[:, at] = sum(dot(own, part) for part in split(spread(drive_im), 2))
+        forward(1 + (n_ep - 1) * s // (2 * spans), 1 + (n_ep - 1) * (s + 1) // (2 * spans))
 
     for s in range(spans):
         at = slice(s * span, (s + 1) * span)
@@ -169,7 +213,6 @@
             packed[r : r + 1, :] = w_re[:, cut]
             packed[rows + r : rows + r + 1, :] = w_im[:, cut]
 
-    pl.semaphore_wait(barrier, n_ep - 1 + n_tp - 1)
     copies = []
     for d in range(1, n_ep):
         copy = pltpu.make_async_remote_copy(
@@ -179,6 +222,7 @@
         )
         copy.start()
         copies.append(copy)
+    forward(1 + (n_ep - 1) // 2, n_ep)
     for copy in copies:
         copy.wait()
     wl_re, wl_im = packed[0:rows, :], packed[rows : 2 * rows, :]
@@ -245,9 +289,99 @@
         copies.append(copy)
     for copy in copies:
         copy.wait()
-
-
-def mixer(inputs, retain, lam_re, lam_im, log_dt, b_re, b_im, c_re, c_im, d_skip):
+    _, value = added(n_ep)
+    home_ref[me] = value
+
+    @pl.loop(1, n_ep)
+    def _(d):
+        home(d).wait()
+
+    @pl.loop(1, n_ep + 1)
+    def _(d):
+        for hop in range(1, n_tp):
+            scatter(d, hop).wait_send()
+
+
+def dispatch_kernel(
+    n_ep, n_tp, rows_ref, got_ref, route_send, route_recv, share_send, share_recv
+):
+    me, mine = lax.axis_index("ep"), lax.axis_index("tp")
+    barrier = pltpu.get_barrier_semaphore()
+    for d in range(1, n_ep):
+        pl.semaphore_signal(
+            barrier, inc=1, device_id=(lax.rem(me + d, n_ep), mine), device_id_type=MESH
+        )
+    for d in range(1, n_tp):
+        pl.semaphore_signal(
+            barrier, inc=1, device_id=(me, lax.rem(mine + d, n_tp)), device_id_type=MESH
+        )
+
+    features = rows_ref.shape[2]
+    columns = pl.ds(pl.multiple_of(mine * features, LANES), features)
+
+    def route(d):
+        return pltpu.make_async_remote_copy(
+            src_ref=rows_ref.at[lax.rem(me + d, n_ep)], dst_ref=got_ref.at[me, :, columns],
+            send_sem=route_send.at[d - 1], recv_sem=route_recv.at[d - 1],
+            device_id=(lax.rem(me + d, n_ep), mine), device_id_type=MESH,
+        )
+
+    def share(d, hop, source=None):
+        sender = lax.rem(me + n_ep - d, n_ep)
+        block = got_ref.at[sender, :, columns]
+        return pltpu.make_async_remote_copy(
+            src_ref=block if source is None else source, dst_ref=block,
+            send_sem=share_send.at[d, hop - 1], recv_sem=share_recv.at[d, hop - 1],
+            device_id=(me, lax.rem(mine + hop, n_tp)), device_id_type=MESH,
+        )
+
+    def forward(low, high):
+        @pl.loop(low, high)
+        def _(d):
+            route(d).wait_recv()
+            for hop in range(1, n_tp):
+                share(d, hop).start()
+
+    pl.semaphore_wait(barrier, n_ep - 1 + n_tp - 1)
+
+    @pl.loop(1, n_ep)
+    def _(d):
+        route(d).start()
+
+    for hop in range(1, n_tp):
+        share(0, hop, rows_ref.at[me]).start()
+    got_ref[me, :, columns] = rows_ref[me]
+    forward(1, n_ep)
+    for hop in range(1, n_tp):
+        share(0, hop, rows_ref.at[me]).wait()
+
+    @pl.loop(1, n_ep)
+    def _(d):
+        route(d).wait_send()
+        for hop in range(1, n_tp):
+            share(d, hop).wait()
+
+
+def dispatch(outgoing):
+    n_ep, n_tp = lax.axis_size("ep"), lax.axis_size("tp")
+    _, slots, features = outgoing.shape
+    dma = pltpu.SemaphoreType.DMA
+    return pl.pallas_call(
+        functools.partial(dispatch_kernel, n_ep, n_tp),
+        out_shape=jax.ShapeDtypeStruct((n_ep, slots, features * n_tp), jnp.bfloat16),
+        in_specs=[pl.BlockSpec(memory_space=pltpu.VMEM)],
+        out_specs=pl.BlockSpec(memory_space=pltpu.VMEM),
+        scratch_shapes=[
+            dma((n_ep - 1,)), dma((n_ep - 1,)), dma((n_ep, n_tp - 1)), dma((n_ep, n_tp - 1)),
+        ],
+        compiler_params=pltpu.CompilerParams(collective_id=1, has_side_effects=True),
+        cost_estimate=pl.CostEstimate(
+            flops=20_000_000_000, bytes_accessed=4_000_000, transcendentals=0
+        ),
+    )(outgoing)
+
+
+def mixer(inputs, retain, lam_re, lam_im, log_dt, b_re, b_im, c_re, c_im, d_skip, partial_out):
     length, here = inputs.shape
     groups, channels, states = c_re.shape
     width = groups * states
@@ -262,13 +396,18 @@
         ]
     ).reshape(4, channels, width)
     rows = width // LANES
+    _, slots, features = partial_out.shape
+    features = features // n_tp
     big = pltpu.VMEM((length, width), jnp.float32)
     dma = pltpu.SemaphoreType.DMA
     return pl.pallas_call(
         functools.partial(mixer_kernel, n_ep, n_tp, (length, groups, states, channels)),
-        out_shape=jax.ShapeDtypeStruct((length, here * n_tp), jnp.bfloat16),
-        in_specs=[pl.BlockSpec(memory_space=pltpu.VMEM)] * 5,
-        out_specs=pl.BlockSpec(memory_space=pltpu.VMEM),
+        out_shape=(
+            jax.ShapeDtypeStruct((length, here * n_tp), jnp.bfloat16),
+            jax.ShapeDtypeStruct((n_ep, slots, features), jnp.bfloat16),
+        ),
+        in_specs=[pl.BlockSpec(memory_space=pltpu.VMEM)] * 6,
+        out_specs=(pl.BlockSpec(memory_space=pltpu.VMEM),) * 2,
         scratch_shapes=[
             big, big, big,
             pltpu.VMEM((5, CHUNKS, width), jnp.float32),
@@ -276,12 +415,15 @@
             pltpu.VMEM((2 * rows, LANES), jnp.float32),
             pltpu.VMEM((n_ep, 3 * rows, LANES), jnp.float32),
             dma((n_ep - 1,)), dma((n_ep - 1,)), dma((n_tp - 1,)), dma((n_tp - 1,)),
+            dma((n_ep - 1,)), dma((n_ep - 1,)), dma((n_ep, n_tp - 1)), dma((n_ep, n_tp - 1)),
+            pltpu.VMEM((n_ep, n_tp - 1, slots, features), jnp.bfloat16),
+            pltpu.VMEM((n_ep, slots, features), jnp.bfloat16),
         ],
         compiler_params=pltpu.CompilerParams(collective_id=0, has_side_effects=True),
         cost_estimate=pl.CostEstimate(
             flops=20_000_000_000, bytes_accessed=4_000_000, transcendentals=0
         ),
-    )(inputs, retain, coef, mats, d_skip.reshape(1, here))
+    )(inputs, retain, coef, mats, d_skip.reshape(1, here), partial_out)
 
 
 def local(
@@ -311,12 +453,6 @@
     own_inputs = lax.dynamic_slice_in_dim(
         normed, lax.axis_index("tp") * channels_here, channels_here, 1
     )
-    piece = mixer(
-        own_inputs, log_retain, lam_re, lam_im, log_dt, b_re, b_im, c_re, c_im, d_skip
-    )
-    mix_lin = jnp.dot(piece, w_lin, preferred_element_type=jnp.float32)
-    mix_glu = jnp.dot(piece, w_glu, preferred_element_type=jnp.float32)
-    mix_out = (mix_lin * jax.nn.sigmoid(mix_glu)).astype(jnp.bfloat16)
     normed_b = root_mean_normed(moe_in, moe_gain)
     experts = lax.axis_size("ep")
     tokens_here, choices_each = routes.shape
@@ -342,22 +478,18 @@
     gate_local = w_gate[0]
     up_local = w_up[0]
     down_local = w_down[0]
-    received = lax.all_to_all(outgoing, "ep", split_axis=0, concat_axis=0, tiled=True)
-    senders, slots_here, features_here = received.shape
-    piece = lax.all_gather(received, "tp", axis=2, tiled=True)
-    piece_rows = piece.reshape(senders * slots_here, piece.shape[2])
+    received = dispatch(outgoing)
+    piece_rows = received.reshape(experts * capacity, received.shape[2])
     gate_pre = jnp.dot(piece_rows, gate_local, preferred_element_type=jnp.float32)
     up_pre = jnp.dot(piece_rows, up_local, preferred_element_type=jnp.float32)
     hidden = (jax.nn.silu(gate_pre) * up_pre).astype(jnp.bfloat16)
     partial_out = jnp.dot(hidden, down_local, preferred_element_type=jnp.float32).astype(
         jnp.bfloat16
     )
-    partial_out = lax.optimization_barrier(partial_out)
-    summed = lax.psum_scatter(
-        partial_out.astype(jnp.float32).astype(jnp.bfloat16), "tp", scatter_dimension=1, tiled=True
-    ).astype(jnp.float32)
-    final_result = summed.astype(jnp.bfloat16).reshape(senders, slots_here, summed.shape[1])
-    returned = lax.all_to_all(final_result, "ep", split_axis=0, concat_axis=0, tiled=True)
+    piece, returned = mixer(
+        own_inputs, log_retain, lam_re, lam_im, log_dt, b_re, b_im, c_re, c_im, d_skip,
+        partial_out.reshape(experts, capacity, partial_out.shape[1]),
+    )
     flat_returned = returned.reshape(experts * capacity, returned.shape[2])
     gathered = (
         flat_returned[target]
@@ -365,6 +497,9 @@
         .reshape(tokens_here, choices_each, returned.shape[2])
     )
     moe_out = jnp.sum(gathered * route_weight[:, :, None], axis=1).astype(jnp.bfloat16)
+    mix_lin = jnp.dot(piece, w_lin, preferred_element_type=jnp.float32)
+    mix_glu = jnp.dot(piece, w_glu, preferred_element_type=jnp.float32)
+    mix_out = (mix_lin * jax.nn.sigmoid(mix_glu)).astype(jnp.bfloat16)
     return (mix_out, moe_out)
 
 

time: 138 us -> 94.3 us (0.68)
  waiting for transfers between devices: 42.1 us -> 0 us
  Pallas kernels: 21.1 us -> 61.4 us
  blocking collectives: 18.9 us -> 0 us
  between operations: 14.3 us -> 0.9 us
  starting transfers between devices: 4.69 us -> 0 us
  other arithmetic: 9.26 us -> 6.25 us
    pallas_call x0 -> x1, Pallas kernels: none -> 27.5 us  [dispatch(): pl.pallas_call(functools.partial(dispatch_kernel, n_ep, n_tp), out_shape=...]
    all_gather x1 -> x0, waiting for transfers between devices: 23.5 us -> none  [local(): piece = lax.all_gather(received, 'tp', axis=2, tiled=True)]
    all_to_all x1 -> x0, blocking collectives: 18.9 us -> none  [local(): lax.all_to_all(outgoing, 'ep', split_axis=0, concat_axis=0, tiled=True)]
    pallas_call x1, Pallas kernels: 21.1 us -> 33.8 us  [mixer(): pl.pallas_call(functools.partial(mixer_kernel, n_ep, n_tp, (length, group...]
    all_to_all x1 -> x0, waiting for transfers between devices: 9.61 us -> none  [local(): lax.all_to_all(final_result, 'ep', split_axis=0, concat_axis=0, tiled=True)]
    reduce_scatter x1 -> x0, waiting for transfers between devices: 8.91 us -> none  [local(): lax.psum_scatter(partial_out.astype(jnp.float32).astype(jnp.bfloat16), 't...]
    all_to_all x1 -> x0, starting transfers between devices: 4.61 us -> none  [local(): lax.all_to_all(final_result, 'ep', split_axis=0, concat_axis=0, tiled=True)]
    convert_element_type x2, other arithmetic: 3.32 us -> 1.23 us  [root_mean_normed(): broadened_rows = values.astype(jnp.float32)]
  transfers between devices with their start and end apart: 3 -> 0, of which waited for: 3 -> 0; matrix products, arithmetic and copies ran while one was open for 9% -> 0% of each run, Pallas kernels for 15% -> 0%
where the time goes in v3:
time: 94.3 us; the launch traced here: 93.9 us
  Pallas kernels  61.4 us (65%)
  matrix products  17.4 us (18%)
  local copies, waits for them, and re-layouts  8.01 us (8%)
  other arithmetic  6.25 us (7%)
    pallas_call x1, Pallas kernels, mixer(): pl.pallas_call(functools.partial(mixer_kernel, n_ep, n_tp, (length, group...  33.8 us
    pallas_call x1, Pallas kernels, dispatch(): pl.pallas_call(functools.partial(dispatch_kernel, n_ep, n_tp), out_shape=...  27.5 us
    dot_general x1, matrix products, local(): jnp.dot(hidden, down_local, preferred_element_type=jnp.float32)  9.08 us
    dot_general x1, matrix products, local(): jnp.dot(piece_rows, gate_local, preferred_element_type=jnp.float32)  5.59 us
    gather x1, local copies, waits for them, and re-layouts, local(): flat_returned[target].astype(jnp.float32)  2.26 us

profile of v3, /device:TPU:0, one launch (start us, length us, event | category | flops | bytes accessed | tf_op | source)
XLA Modules:
  0.0 93.9 jit_solution(15836723461536736985)
XLA Ops:
  0.6 0.0 copy-start
  0.6 0.0 copy-start.1
  0.7 0.9 %copy.42 = s32[128,2]{1,0:T(8,128)S(1)} copy(s32[128,2]{0,1:T(2,128)} %param.35) | data formatting | bytes 2048 | tf_op args[15]
  1.6 0.1 eq.43
  1.8 0.6 reduce-window.6
  2.3 0.2 slice_reduce_fusion
  2.6 0.1 eq.39
  2.7 0.1 fusion.31
  2.8 0.1 reduce_sum.42
  3.0 0.1 copy.45
  3.1 0.1 fusion.19
  3.1 0.8 dynamic-slice.1
  3.9 1.1 %convert_element_type.46 = f32[128,2048]{1,0:T(8,128)S(1)} convert(bf16[128,2048]{1,0:T(8,128)(2,1)} %param.33) | non-fusion elementwise | flops 262144 | bytes 1572864 | tf_op jit(solution)/shard_map/convert_element_type | solution.py:14
  5.0 0.0 copy-done.1
  5.1 0.2 multiply_reduce_fusion
  5.3 1.1 %convolution_convert_fusion = bf16[384,512]{1,0:T(8,128)(2,1)} fusion(pred[384,128]{1,0:T(8,128)(4,1)S(1)} %fusion.19, f32[128,2048]{1,0:T(8,128)S(1)} %convert_element_type.46, s32[]{:T(128)S(6)} %select_n.14, f32[512]{0:T(512)S(1)} %dynamic-slice.1, f32[128]{0:T(128)S(1)} %add_rsqrt_fusion), kind=kOutput, calls=%fused_computation.9 | convolution fusion | flops 50724864 | bytes 707076 | tf_op jit(solution)/shard_map/dot_general | solution.py:476
  6.3 27.5 %shard_map.203 = bf16[8,48,2048]{2,1,0:T(8,128)(2,1)} custom-call(bf16[8,48,512]{2,1,0:T(8,128)(2,1)} %bitcast.42), custom_call_target="tpu_custom_call" | custom-call | flops 20000000000 | bytes 4000000 | tf_op jit(solution)/shard_map/pallas_call | solution.py:369
  33.9 5.6 %fusion.4 = f32[384,1024]{1,0:T(8,128)} fusion(bf16[384,2048]{1,0:T(8,128)(2,1)} %bitcast.51, bf16[1,2048,1024]{2,1,0:T(8,128)(2,1)} %param.37), kind=kOutput, calls=%fused_computation.5 | convolution fusion | flops 1610612736 | bytes 7340032 | tf_op jit(solution)/shard_map/dot_general | solution.py:483
  39.5 9.1 %fusion.6 = bf16[384,2048]{1,0:T(8,128)(2,1)} fusion(bf16[1,1024,2048]{2,1,0:T(8,128)(2,1)} %param.39, f32[384,1024]{1,0:T(8,128)} %fusion.4, bf16[384,2048]{1,0:T(8,128)(2,1)} %bitcast.52, bf16[1,2048,1024]{2,1,0:T(8,128)(2,1)} %param.38), kind=kOutput, calls=%fused_computation.7 | convolution fusion | flops 3224371200 | bytes 13107200 | tf_op jit(solution)/shard_map/dot_general | solution.py:486
  48.6 0.0 copy-start.5
  48.6 0.8 dynamic-slice
  49.4 0.0 copy-done.2
  49.4 0.1 convert_element_type.42
  49.5 0.2 multiply_reduce_fusion.1
  49.7 0.8 fusion.23.u_ref
  50.5 0.0 copy-done.13
  50.5 0.0 copy-done.9
  50.5 0.0 copy-done.10
  50.5 0.2 fusion.28
  50.7 0.1 stack.30
  50.8 0.1 stack.31
  50.9 0.1 stack.32
  50.9 0.1 stack.33
  51.0 0.6 pad_maximum_fusion.1.coef_ref
  51.7 0.0 copy-done.4
  51.7 0.1 copy.38
  51.8 0.0 copy-start.8
  51.8 0.1 stack.35
  51.9 0.0 copy-done.5
  51.9 0.1 copy.39
  52.0 0.1 stack.36
  52.1 0.0 copy-done.6
  52.1 0.1 copy.40
  52.2 0.1 stack.37
  52.3 0.0 copy-done.7
  52.3 0.1 copy.41
  52.4 0.1 stack.38
  52.5 0.8 pad_maximum_fusion.mats_ref
  53.4 0.0 copy-done.8
  53.4 0.7 copy.46.keep_ref
  54.1 33.8 %shard_map.204 = (bf16[128,2048]{1,0:T(8,128)(2,1)}, bf16[8,48,512]{2,1,0:T(8,128)(2,1)}) custom-call(bf16[128,512]{1,0:T(8,128)(2,1)} %fusion.23.u_ref, f32[128,32]{1,0:T(8,128)} %copy.46.keep_ref, f32[4,2048]{1,0:T(4,128)} %pad_maximum_fusion.1.coef_ref, f32[4,16,2048]{2,1,0:T(8,128)} %pad_maximum_fusion.mats_ref, f32[1,512]{1,0:T(1,128)} %bitcast.49, ...), custom_call_target="tpu_custom_call" | custom-call | flops 20000000000 | bytes 4000000 | tf_op jit(solution)/shard_map/pallas_call | solution.py:403
  88.0 0.0 copy-start.11
  88.0 0.0 copy-start.3
  88.0 0.1 mul.172
  88.2 2.3 %gather_fusion = bf16[256,512]{1,0:T(8,128)(2,1)S(1)} fusion(bf16[384,512]{1,0:T(8,128)(2,1)} %bitcast.41, s32[1024]{0:T(1024)S(1)} %pad_clamp_fusion), kind=kCustom, calls=%fused_computation | custom fusion | bytes 525312 | tf_op jit(solution)/shard_map/gather | solution.py:495
  90.4 0.3 reshape.119
  90.8 0.0 copy-done.11
  90.8 0.1 copy.47
  90.9 1.4 %multiply_reduce_fusion.2 = bf16[128,512]{1,0:T(8,128)(2,1)} fusion(f32[128,2,512]{2,1,0:T(2,128)S(1)} %reshape.119, f32[128,2]{1,0:T(8,128)S(1)} %copy.47), kind=kLoop, calls=%fused_computation.20 | loop fusion | flops 196608 | bytes 656384 | tf_op jit(solution)/shard_map/reduce_sum | solution.py:499
  92.3 0.0 copy-done
  92.3 0.0 copy-done.3
  92.3 0.4 fusion.36
  92.7 0.0 copy-done.12
  92.7 1.2 %fusion.15 = bf16[128,512]{1,0:T(8,128)(2,1)} fusion(f32[128,512]{1,0:T(8,128)S(1)} %fusion.36, bf16[128,2048]{1,0:T(8,128)(2,1)S(1)} %copy-done.3, bf16[2048,512]{1,0:T(8,128)(2,1)S(1)} %copy-done.12), kind=kOutput, calls=%fused_computation.15 | convolution fusion | flops 268763136 | bytes 3014656 | tf_op jit(solution)/shard_map/dot_general | solution.py:501
  (17 shorter events, 0.1 us)
Async XLA Ops:
  0.6 91.6 %copy-start = (bf16[2048,512]{1,0:T(8,128)(2,1)S(1)}, bf16[2048,512]{1,0:T(8,128)(2,1)}, u32[]{:S(2)}) copy-start(bf16[2048,512]{1,0:T(8,128)(2,1)} %param.31) | copy-start | bytes 6291460
  0.6 4.4 %copy-start.1 = (bf16[128,2048]{1,0:T(8,128)(2,1)S(1)}, bf16[128,2048]{1,0:T(8,128)(2,1)}, u32[]{:S(2)}) copy-start(bf16[128,2048]{1,0:T(8,128)(2,1)} %param.33) | copy-start | bytes 1572868
  39.5 9.9 %copy-start.2 = (bf16[128,2048]{1,0:T(8,128)(2,1)S(1)}, bf16[128,2048]{1,0:T(8,128)(2,1)}, u32[]{:S(2)}) copy-start(bf16[128,2048]{1,0:T(8,128)(2,1)} %param.20) | copy-start | bytes 1572868
  48.5 1.9 %copy-start.13 = (f32[32]{0:T(128)S(1)}, f32[32]{0:T(128)}, u32[]{:S(2)}) copy-start(f32[32]{0:T(128)} %param.24) | copy-start | bytes 388
  48.5 1.9 %copy-start.9 = (f32[32,64]{1,0:T(8,128)S(1)}, f32[32,64]{1,0:T(8,128)}, u32[]{:S(2)}) copy-start(f32[32,64]{1,0:T(8,128)} %param.23) | copy-start | bytes 24580
  48.5 1.9 %copy-start.10 = (f32[32,64]{1,0:T(8,128)S(1)}, f32[32,64]{1,0:T(8,128)}, u32[]{:S(2)}) copy-start(f32[32,64]{1,0:T(8,128)} %param.22) | copy-start | bytes 24580
  48.5 3.1 %copy-start.4 = (f32[32,64,16]{1,2,0:T(8,128)S(1)}, f32[32,64,16]{1,2,0:T(8,128)}, u32[]{:S(2)}) copy-start(f32[32,64,16]{1,2,0:T(8,128)} %param.25) | copy-start | bytes 393220
  48.6 3.3 %copy-start.5 = (f32[32,64,16]{1,2,0:T(8,128)S(1)}, f32[32,64,16]{1,2,0:T(8,128)}, u32[]{:S(2)}) copy-start(f32[32,64,16]{1,2,0:T(8,128)} %param.26) | copy-start | bytes 393220
  49.4 2.7 %copy-start.6 = (f32[32,16,64]{2,1,0:T(8,128)S(1)}, f32[32,16,64]{2,1,0:T(8,128)}, u32[]{:S(2)}) copy-start(f32[32,16,64]{2,1,0:T(8,128)} %param.27) | copy-start | bytes 393220
  49.7 2.6 %copy-start.7 = (f32[32,16,64]{2,1,0:T(8,128)S(1)}, f32[32,16,64]{2,1,0:T(8,128)}, u32[]{:S(2)}) copy-start(f32[32,16,64]{2,1,0:T(8,128)} %param.28) | copy-start | bytes 393220
  51.8 1.6 %copy-start.8 = (f32[128,32]{0,1:T(8,128)S(1)}, f32[128,32]{0,1:T(8,128)}, u32[]{:S(2)}) copy-start(f32[128,32]{0,1:T(8,128)} %param.30) | copy-start | bytes 49156
  88.0 2.8 %copy-start.11 = (f32[128,2]{0,1:T(2,128)S(1)}, f32[128,2]{0,1:T(2,128)}, u32[]{:S(2)}) copy-start(f32[128,2]{0,1:T(2,128)} %param.36) | copy-start | bytes 3076
  88.0 4.3 %copy-start.3 = (bf16[128,2048]{1,0:T(8,128)(2,1)S(1)}, bf16[128,2048]{1,0:T(8,128)(2,1)}, u32[]{:S(2)}) copy-start(bf16[128,2048]{1,0:T(8,128)(2,1)} %get-tuple-element.4) | copy-start | bytes 1572868
  90.9 1.8 %copy-start.12 = (bf16[2048,512]{1,0:T(8,128)(2,1)S(1)}, bf16[2048,512]{1,0:T(8,128)(2,1)}, u32[]{:S(2)}) copy-start(bf16[2048,512]{1,0:T(8,128)(2,1)} %param.32) | copy-start | bytes 6291460
